TPU v7x, 32 devices: a whole 2x2x4 slice. The times are simulated.
32 devices in a mesh: grp: 2 (over y), sp: 4 (over z), tp: 4 (over x, core).
Axes of the slice: x: 2, y: 2, z: 4, core: 2. Of those that a mesh axis runs over, the one named last changes fastest.
Arguments:
- hidden_in: bfloat16 [3072, 4096], P(('grp', 'sp'), 'tp'), parts along dimension 0, may hold values from -30 to 30
- in_gain: float32 [2, 4096], P(None, 'tp'), may hold values from 0.1 to 1.9
- w_value: bfloat16 [2, 4096, 2048], P(None, 'sp', 'tp'), may hold values from -0.09375 to 0.09375
- w_gate: bfloat16 [2, 4096, 2048], P(None, 'sp', 'tp'), may hold values from -0.09375 to 0.09375
- conv_taps: float32 [2, 31, 2048], P(None, None, 'tp'), may hold values from -9 to 9
- norm_gain: float32 [2, 2048], P(None, 'tp'), may hold values from 0.1 to 1.9
- norm_shift: float32 [2, 2048], P(None, 'tp'), may hold values from -3 to 3
- w_out: bfloat16 [2, 2048, 4096], P(None, 'tp', 'sp'), may hold values from -0.125 to 0.125
Outputs:
- hidden_out: bfloat16 [3072, 4096], P(('grp', 'sp'), 'tp'), parts along dimension 0
There are 2 independent parts, one for each index of `grp`. A program takes and returns all parts, laid end to end along the dimension named above; an argument that names none is the same for every part. Nothing has to cross between parts.
All inputs are finite; a program needn't handle non-finite values.
Results may differ from a plain program's by a relative error of at most 0.013.
Values may be sent and summed in bfloat16 or wider, within the bound.
A program may use at most 64 MiB of HBM per device.

v0:
```python
import functools

import jax
import jax.numpy as jnp
from jax import lax
from jax.experimental import pallas as pl
from jax.experimental.pallas import tpu as pltpu
from jax.sharding import PartitionSpec as P

epsilon = 1e-06
CHUNK = 128
F32, BF16 = jnp.float32, jnp.bfloat16


def kernel(
    S, T, h_ref, gain_ref, wv_ref, wg_ref, taps_ref, ng_ref, ns_ref, wo_ref, out_ref,
    WV, WG, WO, X, ACC, EXT, CONV, MIX, PART, PRECV, SUMB, RECV, STAT, HB,
    own_sem, zr, zs_right, zs_left, yr, ys, xr, xs, xf, sr, ss, hr, hs, pr, ps, rr, rs,
):
    L = wv_ref.shape[0]
    Ds, Cn = wv_ref.shape[1], wv_ref.shape[2]
    rows, Dt = h_ref.shape
    taps = taps_ref.shape[1]
    features, channels = Dt * T, Cn * T
    chips = T // 2
    halo = EXT.shape[1] - rows
    g, me, t = lax.axis_index("grp"), lax.axis_index("sp"), lax.axis_index("tp")
    core = lax.rem(t, 2)
    chip = lax.div(t, 2)
    partner = t + 1 - 2 * core
    MESH = pl.DeviceIdType.MESH
    first, last = me == 0, me == S - 1

    sources = [(wv_ref, WV), (wg_ref, WG), (wo_ref, WO)]

    def own(layer, which):
        source, slots = sources[which]
        return pltpu.make_async_copy(source.at[layer], slots.at[layer, me], own_sem.at[layer, which])

    for layer in range(L):
        for which in range(3):
            own(layer, which).start()

    def each_chunk(body, size=CHUNK):
        def step(index, _):
            body(pl.ds(pl.multiple_of(index * size, size), size))
            return 0

        lax.fori_loop(0, rows // size, step, 0)

    def put_stat(slot, where, left, right):
        lane = lax.broadcasted_iota(jnp.int32, (left.shape[0], 128), 1)
        wide = jnp.where(lane == 0, left, right)
        STAT[slot, t, :, where] = wide.T[:8]

    def stat_copy(slot, peer):
        return pltpu.make_async_remote_copy(
            STAT.at[slot, t], STAT.at[slot, t], ss.at[slot, peer], sr.at[slot, t],
            device_id={"tp": peer}, device_id_type=MESH,
        )

    def stat_arrival(slot, peer):
        return pltpu.make_async_remote_copy(
            STAT.at[slot, peer], STAT.at[slot, peer], ss.at[slot, peer], sr.at[slot, peer],
            device_id={"tp": peer}, device_id_type=MESH,
        )

    def send_stat(slot):
        for shift in range(1, T):
            stat_copy(slot, lax.rem(t + shift, T)).start()

    def wait_stat(slot):
        for shift in range(1, T):
            stat_arrival(slot, lax.rem(t + shift, T)).wait_recv()

    def get_stat(slot, where):
        total = STAT[slot, 0, :, where]
        for peer in range(1, T):
            total = total + STAT[slot, peer, :, where]
        return jnp.concatenate([total] * 16, axis=0).T

    def half_ref(item, owner):
        kind, layer = item % 4, item // 4
        if kind < 2:
            size = Ds // 2
            return (WV, WG)[kind].at[layer, owner, pl.ds(pl.multiple_of(g * size, size), size)]
        size = Cn // 4
        start = pl.multiple_of(g * (2 * size) + (kind - 2) * size, size)
        return WO.at[layer, owner, pl.ds(start, size)]

    def other_ref(item, owner):
        kind, layer = item % 4, item // 4
        if kind < 2:
            size = Ds // 2
            return (WV, WG)[kind].at[layer, owner, pl.ds(pl.multiple_of((1 - g) * size, size), size)]
        size = Cn // 4
        start = pl.multiple_of((1 - g) * (2 * size) + (kind - 2) * size, size)
        return WO.at[layer, owner, pl.ds(start, size)]

    def zcopy(item, owner, way):
        ref = half_ref(item, owner)
        sems = zs_right if way > 0 else zs_left
        return pltpu.make_async_remote_copy(
            ref, ref, sems.at[item, owner], zr.at[item, owner],
            device_id={"sp": me + way}, device_id_type=MESH,
        )

    def ycopy(item, owner):
        ref = half_ref(item, owner)
        return pltpu.make_async_remote_copy(
            ref, ref, ys.at[item, owner], yr.at[item, owner],
            device_id={"grp": 1 - g}, device_id_type=MESH,
        )

    def yarrival(item, owner):
        ref = other_ref(item, owner)
        return pltpu.make_async_remote_copy(
            ref, ref, ys.at[item, owner], yr.at[item, owner],
            device_id={"grp": 1 - g}, device_id_type=MESH,
        )

    def event(item, k):
        if k == 0:
            if item % 4 < 3:
                own(item // 4, item % 4).wait()

            @pl.when(jnp.logical_not(last))
            def _():
                zcopy(item, me, 1).start()

            @pl.when(jnp.logical_not(first))
            def _():
                zcopy(item, me, -1).start()

            return

        @pl.when(me - k >= 0)
        def _():
            owner = me - k
            zcopy(item, owner, 1).wait_recv()

            @pl.when(jnp.logical_not(last))
            def _():
                zcopy(item, owner, 1).start()

            ycopy(item, owner).start()

        @pl.when(me + k < S)
        def _():
            owner = me + k
            zcopy(item, owner, -1).wait_recv()

            @pl.when(jnp.logical_not(first))
            def _():
                zcopy(item, owner, -1).start()

            ycopy(item, owner).start()

    def xcopy(layer, source, peer, sem):
        return pltpu.make_async_remote_copy(
            X.at[layer, source], X.at[layer, source], sem, xr.at[layer, source],
            device_id={"tp": peer}, device_id_type=MESH,
        )

    def make_x(layer):
        source = h_ref if layer == 0 else HB

        def body(where):
            wide = source[where, :].astype(F32)
            X[layer, t, where, :] = (wide * gain_ref[layer : layer + 1, :]).astype(BF16)
            squares = jnp.sum(wide * wide, axis=1, keepdims=True)
            put_stat(2 * layer, where, squares, squares)

        each_chunk(body)

    def send_x(layer):
        for shift in range(1, chips):
            peer = lax.rem(chip + shift, chips) * 2 + core
            xcopy(layer, t, peer, xs.at[layer, shift]).start()
        xcopy(layer, t, partner, xs.at[layer, 0]).start()
        send_stat(2 * layer)

    def relay_x(layer):
        for shift in range(1, chips):
            source = lax.rem(chip + shift, chips) * 2 + core
            xcopy(layer, source, partner, xf.at[layer, shift]).wait_recv()
            xcopy(layer, source, partner, xf.at[layer, shift]).start()

    def wait_x(layer):
        for shift in range(chips):
            source = lax.rem(chip + shift, chips) * 2 + 1 - core
            xcopy(layer, source, partner, xf.at[layer, 0]).wait_recv()
        wait_stat(2 * layer)

    def by_arrival(body):
        def step(turn, _):
            away = lax.div(turn + 1, 2)
            owner = jnp.where(lax.rem(turn, 2) == 1, me + away, me - away)

            @pl.when(jnp.logical_and(owner >= 0, owner < S))
            def _():
                body(turn, owner)

            return 0

        lax.fori_loop(0, 2 * S - 1, step, 0)

    def project(layer):
        def block(turn, owner):
            @pl.when(turn > 0)
            def _():
                yarrival(4 * layer, owner).wait_recv()
                yarrival(4 * layer + 1, owner).wait_recv()

            at = lax.div(owner * Ds, Dt)
            columns = pl.ds(pl.multiple_of(lax.rem(owner * Ds, Dt), 128), Ds)
            xs_block = X[layer, at, :, columns]
            for which, slots in ((0, WV), (1, WG)):
                part = jnp.dot(xs_block, slots[layer, owner], preferred_element_type=F32)

                @pl.when(turn == 0)
                def _():
                    ACC[which] = part

                @pl.when(turn > 0)
                def _():
                    ACC[which] += part

        by_arrival(block)

    def halo_copy(layer):
        return pltpu.make_async_remote_copy(
            EXT.at[layer, pl.ds(rows, halo)], EXT.at[layer, pl.ds(0, halo)], hs.at[layer], hr.at[layer],
            device_id={"sp": me + 1}, device_id_type=MESH,
        )

    def gate(layer):
        def body(where):
            mean = get_stat(2 * layer, where)[:, :1] / features
            inv = lax.rsqrt(mean + epsilon)
            value, gating = ACC[0, where, :] * inv, ACC[1, where, :] * inv
            gated = (value / (1.0 + jnp.exp(-gating))).astype(BF16).astype(F32)
            EXT[layer, pl.ds(pl.multiple_of(where.start + halo, 8), where.size), :] = gated

        each_chunk(body)

        @pl.when(jnp.logical_not(last))
        def _():
            halo_copy(layer).start()

        @pl.when(first)
        def _():
            EXT[layer, pl.ds(0, halo), :] = jnp.zeros((halo, Cn), F32)

    def convolve(layer):
        @pl.when(jnp.logical_not(first))
        def _():
            halo_copy(layer).wait_recv()

        tall = CHUNK + halo + 8
        offset = halo - (taps - 1)

        def body(where):
            for column in range(0, Cn, 128):
                at = pl.ds(column, 128)
                tile = jnp.concatenate(
                    [EXT[layer, pl.ds(where.start, CHUNK + halo), at], jnp.zeros((8, 128), F32)], axis=0
                )
                total = jnp.zeros((CHUNK, 128), F32)
                for residue in range(8):
                    ks = [k for k in range(taps) if (k + offset) % 8 == residue]
                    if not ks:
                        continue
                    turned = pltpu.roll(tile, tall - residue, 0) if residue else tile
                    for k in ks:
                        low = k + offset - residue
                        total = total + taps_ref[layer, k : k + 1, at] * turned[low : low + CHUNK]
                CONV[where, at] = total
            conved = CONV[where, :]
            put_stat(
                2 * layer + 1, where,
                jnp.sum(conved, axis=1, keepdims=True),
                jnp.sum(conved * conved, axis=1, keepdims=True),
            )

        each_chunk(body)
        send_stat(2 * layer + 1)

    def mix(layer):
        wait_stat(2 * layer + 1)

        def body(where):
            stat = get_stat(2 * layer + 1, where)
            mean = stat[:, 0:1] / channels
            spread = stat[:, 1:2] / channels - mean * mean
            normed = (CONV[where, :] - mean) * lax.rsqrt(spread + epsilon) * ng_ref[
                layer : layer + 1, :
            ] + ns_ref[layer : layer + 1, :]
            MIX[where, :] = (normed / (1.0 + jnp.exp(-normed))).astype(BF16)

        each_chunk(body)

    def pair_copy(layer, at):
        return pltpu.make_async_remote_copy(
            PART.at[layer, 2 * at + 1 - core], PRECV.at[layer, at], ps.at[layer, at], pr.at[layer, at],
            device_id={"tp": partner}, device_id_type=MESH,
        )

    def sum_copy(layer, at):
        return pltpu.make_async_remote_copy(
            SUMB.at[layer, at], RECV.at[layer, chip], rs.at[layer, at], rr.at[layer, chip],
            device_id={"tp": at * 2 + core}, device_id_type=MESH,
        )

    def sum_arrival(layer, at):
        return pltpu.make_async_remote_copy(
            SUMB.at[layer, at], RECV.at[layer, at], rs.at[layer, at], rr.at[layer, at],
            device_id={"tp": at * 2 + core}, device_id_type=MESH,
        )

    def sum_pair(layer, at):
        pair_copy(layer, at).wait_recv()

        def body(where):
            SUMB[layer, at, where, :] = (
                PART[layer, at * 2 + core, where, :].astype(F32) + PRECV[layer, at, where, :].astype(F32)
            ).astype(BF16)

        each_chunk(body)
        sum_copy(layer, at).start()

    def branch(layer):
        def block(turn, owner):
            @pl.when(turn > 0)
            def _():
                yarrival(4 * layer + 2, owner).wait_recv()
                yarrival(4 * layer + 3, owner).wait_recv()

            target = lax.div(owner * Ds, Dt)
            columns = pl.ds(pl.multiple_of(lax.rem(owner * Ds, Dt), 128), Ds)
            PART[layer, target, :, columns] = jnp.dot(
                MIX[...], WO[layer, owner], preferred_element_type=F32
            ).astype(BF16)
            if S == T:
                at = lax.div(target, 2)

                @pl.when(lax.rem(target, 2) != core)
                def _():
                    pair_copy(layer, at).start()

                @pl.when(jnp.logical_and(lax.rem(target, 2) == core, at != chip))
                def _():
                    sum_pair(layer, at)

        by_arrival(block)
        if S != T:
            for shift in list(range(1, chips)) + [0]:
                pair_copy(layer, lax.rem(chip + shift, chips)).start()
            for shift in range(1, chips):
                sum_pair(layer, lax.rem(chip + shift, chips))

    def finish(layer):
        pair_copy(layer, chip).wait_recv()
        for shift in range(1, chips):
            sum_arrival(layer, lax.rem(chip + shift, chips)).wait_recv()
        source = h_ref if layer == 0 else HB
        target = out_ref if layer == L - 1 else HB

        def body(where):
            total = PART[layer, t, where, :].astype(F32) + PRECV[layer, chip, where, :].astype(F32)
            for shift in range(1, chips):
                total = total + RECV[layer, lax.rem(chip + shift, chips), where, :].astype(F32)
            target[where, :] = (source[where, :].astype(F32) + total).astype(BF16)

        each_chunk(body)

    barrier = pltpu.get_barrier_semaphore()
    for shift in range(1, T):
        pl.semaphore_signal(barrier, inc=1, device_id={"tp": lax.rem(t + shift, T)}, device_id_type=MESH)
    pl.semaphore_signal(barrier, inc=1, device_id={"grp": 1 - g}, device_id_type=MESH)

    @pl.when(jnp.logical_not(first))
    def _():
        pl.semaphore_signal(barrier, inc=1, device_id={"sp": me - 1}, device_id_type=MESH)

    @pl.when(jnp.logical_not(last))
    def _():
        pl.semaphore_signal(barrier, inc=1, device_id={"sp": me + 1}, device_id_type=MESH)

    inner = jnp.where(first, 0, 1) + jnp.where(last, 0, 1)
    pl.semaphore_wait(barrier, T + inner)

    event(0, 0)
    event(1, 0)
    make_x(0)
    send_x(0)

    def pumped(items, stages, start=1):
        for k in range(start, S):
            for item in items:
                event(item, k)
            if stages:
                stages.pop(0)()
        for stage in stages:
            stage()

    stages = [functools.partial(relay_x, 0), functools.partial(wait_x, 0)]
    ahead = 1
    for layer in range(L):
        base = 4 * layer
        if ahead > 1:
            event(base + 1, 1)
        pumped([base, base + 1], stages, ahead)
        event(base + 2, 0)
        event(base + 3, 0)
        event(base + 2, 1)
        event(base + 3, 1)
        if layer + 1 < L:
            event(base + 4, 0)
        project(layer)
        gate(layer)
        pumped(
            [base + 2, base + 3],
            [functools.partial(convolve, layer), functools.partial(mix, layer)],
            2,
        )
        if layer + 1 < L:
            event(base + 5, 0)
            event(base + 4, 1)
            ahead = 2
        branch(layer)
        if layer + 1 < L:

            def next_x(layer=layer):
                finish(layer)
                make_x(layer + 1)
                send_x(layer + 1)

            def arrive_x(layer=layer):
                relay_x(layer + 1)
                wait_x(layer + 1)

            stages = [next_x, arrive_x]
        else:
            finish(layer)

    for item in range(4 * L):

        def drain(owner, _, item=item):
            @pl.when(jnp.logical_and(owner <= me, jnp.logical_not(last)))
            def _():
                zcopy(item, owner, 1).wait_send()

            @pl.when(jnp.logical_and(owner >= me, jnp.logical_not(first)))
            def _():
                zcopy(item, owner, -1).wait_send()

            @pl.when(owner != me)
            def _():
                ycopy(item, owner).wait_send()

            return 0

        lax.fori_loop(0, S, drain, 0)
    for layer in range(L):
        for slot in (2 * layer, 2 * layer + 1):
            for shift in range(1, T):
                stat_copy(slot, lax.rem(t + shift, T)).wait_send()
        for shift in range(chips):
            xcopy(layer, t, partner, xs.at[layer, shift]).wait_send()
            pair_copy(layer, lax.rem(chip + shift, chips)).wait_send()
        for shift in range(1, chips):
            xcopy(layer, t, partner, xf.at[layer, shift]).wait_send()
            sum_copy(layer, lax.rem(chip + shift, chips)).wait_send()

        @pl.when(jnp.logical_not(last))
        def _(layer=layer):
            halo_copy(layer).wait_send()


def shards(hidden_in, in_gain, w_value, w_gate, conv_taps, norm_gain, norm_shift, w_out):
    S, T = lax.axis_size("sp"), lax.axis_size("tp")
    L, Ds, Cn = w_value.shape
    rows, Dt = hidden_in.shape
    chips = T // 2
    halo = (conv_taps.shape[1] - 1 + 7) // 8 * 8
    vmem = pl.BlockSpec(memory_space=pltpu.VMEM)
    hbm = pl.BlockSpec(memory_space=pl.ANY)
    dma = pltpu.SemaphoreType.DMA
    return pl.pallas_call(
        functools.partial(kernel, S, T),
        out_shape=jax.ShapeDtypeStruct((rows, Dt), BF16),
        in_specs=[vmem, vmem, hbm, hbm, vmem, vmem, vmem, hbm],
        out_specs=vmem,
        scratch_shapes=[
            pltpu.VMEM((L, S, Ds, Cn), BF16),
            pltpu.VMEM((L, S, Ds, Cn), BF16),
            pltpu.VMEM((L, S, Cn, Ds), BF16),
            pltpu.VMEM((L, T, rows, Dt), BF16),
            pltpu.VMEM((2, rows, Cn), F32),
            pltpu.VMEM((L, rows + halo, Cn), F32),
            pltpu.VMEM((rows, Cn), F32),
            pltpu.VMEM((rows, Cn), BF16),
            pltpu.VMEM((L, T, rows, Dt), BF16),
            pltpu.VMEM((L, chips, rows, Dt), BF16),
            pltpu.VMEM((L, chips, rows, Dt), BF16),
            pltpu.VMEM((L, chips, rows, Dt), BF16),
            pltpu.VMEM((2 * L, T, 8, rows), F32),
            pltpu.VMEM((rows, Dt), BF16),
            dma((L, 3)),
            dma((4 * L, S)), dma((4 * L, S)), dma((4 * L, S)), dma((4 * L, S)), dma((4 * L, S)),
            dma((L, T)), dma((L, chips)), dma((L, chips)),
            dma((2 * L, T)), dma((2 * L, T)),
            dma((L,)), dma((L,)),
            dma((L, chips)), dma((L, chips)),
            dma((L, chips)), dma((L, chips)),
        ],
        compiler_params=pltpu.CompilerParams(
            collective_id=0, has_side_effects=True, vmem_limit_bytes=64_000_000
        ),
    )(hidden_in, in_gain, w_value, w_gate, conv_taps, norm_gain, norm_shift, w_out)


def solution(mesh):
    placed = (
        P(("grp", "sp"), "tp"),
        P(None, "tp"),
        P(None, "sp", "tp"),
        P(None, "sp", "tp"),
        P(None, None, "tp"),
        P(None, "tp"),
        P(None, "tp"),
        P(None, "tp", "sp"),
    )
    return jax.shard_map(
        shards, mesh=mesh, in_specs=placed, out_specs=P(("grp", "sp"), "tp"), check_vma=False
    )
```

profile of v0, /device:TPU:3, one launch (start us, length us, event | category | flops | bytes accessed | tf_op | source)
XLA Modules:
  0.0 246.4 jit_solution(10247928322247583299)
XLA Ops:
  0.0 1.6 copy.9.taps_ref
  1.6 242.7 %shard_map.82 = bf16[384,1024]{1,0:T(8,128)(2,1)} custom-call(bf16[384,1024]{1,0:T(8,128)(2,1)} %h_ref.1, f32[2,1024]{1,0:T(2,128)} %gain_ref.1, bf16[2,1024,512]{2,1,0:T(8,128)(2,1)} %wv_ref.1, bf16[2,1024,512]{2,1,0:T(8,128)(2,1)} %wg_ref.1, f32[2,31,512]{2,1,0:T(8,128)} %copy.9.taps_ref, f32[2,512]{1,0:T(2,128)} %ng_ref.1, f32[2,512]{1,0:T(2,128)} %ns_ref.1, ...), custom_call_target="tpu_custom_call" | custom-call | tf_op jit(solution)/shard_map/pallas_call | solution.py:490
  244.3 2.1 copy.11
where the time goes:
time: 247 us; the launch traced here: 246 us
  Pallas kernels  243 us (98%)
  local copies, waits for them, and re-layouts  3.65 us (1%)
    pallas_call x1, Pallas kernels, shards(): pl.pallas_call(functools.partial(kernel, S, T), out_shape=jax.ShapeDtypeS...  243 us

commit v1 on v0

v1 whole, which is shorter than its diff:
```python
import functools

import jax
import jax.numpy as jnp
from jax import lax
from jax.experimental import pallas as pl
from jax.experimental.pallas import tpu as pltpu
from jax.sharding import PartitionSpec as P

epsilon = 1e-06
CHUNK = 128
PIECES = (1, 1, 2)
F32, BF16 = jnp.float32, jnp.bfloat16


def kernel(
    S, T, h_ref, gain_ref, wv_ref, wg_ref, taps_ref, ng_ref, ns_ref, wo_ref, out_ref,
    WV, WG, WO, X, XG, ACC, GACC, EXT, CONV, MIX, PART, PRECV, SUMB, RECV, STAT, GSTAT, HB,
    own_sem, zr, zs_right, zs_left, yr, ys, dr, ds, xr, xs, xf, sr, ss, gr, gs, hr, hs, br, bs,
    pr, ps, rr, rs,
):
    L = wv_ref.shape[0]
    Ds, Cn = wv_ref.shape[1], wv_ref.shape[2]
    rows, Dt = h_ref.shape
    taps = taps_ref.shape[1]
    features, channels = Dt * T, Cn * T
    chips = T // 2
    halo = EXT.shape[1] - 2 * rows
    g, me, t = lax.axis_index("grp"), lax.axis_index("sp"), lax.axis_index("tp")
    core = lax.rem(t, 2)
    chip = lax.div(t, 2)
    partner = t + 1 - 2 * core
    MESH = pl.DeviceIdType.MESH
    both, either, no = jnp.logical_and, jnp.logical_or, jnp.logical_not
    first, last = me == 0, me == S - 1
    low, high = me == 1, me == S - 2
    edge, near = either(first, last), either(low, high)
    inward = jnp.where(first, 1, -1)
    outward = jnp.where(low, -1, 1)
    own_base = jnp.where(low, rows, 0)
    guest_base = jnp.where(low, 0, rows)

    def is_edge(plane):
        return either(plane == 0, plane == S - 1)

    table = []
    groups = []
    for layer in range(L):
        of_layer = []
        for which in range(3):
            ids = []
            for piece in range(PIECES[which]):
                ids.append(len(table))
                table.append((layer, which, piece, PIECES[which]))
            of_layer.append(ids)
        groups.append(of_layer)
    items = len(table)

    def direct(item):
        layer, which, _, _ = table[item]
        return (layer, which) != (0, 2)

    def folded(item):
        layer, which, _, _ = table[item]
        return layer == 0 and which < 2

    def inside(item, plane):
        low_end, high_end = (1, S - 2) if folded(item) else (0, S - 1)
        return both(plane >= low_end, plane <= high_end)

    def skips_y(item, owner):
        if not direct(item):
            return jnp.bool_(False)
        return either(both(owner == 0, low), both(owner == S - 1, high))

    sources = [(wv_ref, WV), (wg_ref, WG), (wo_ref, WO)]

    def own(layer, which):
        source, slots = sources[which]
        return pltpu.make_async_copy(source.at[layer], slots.at[layer, me], own_sem.at[layer, which])

    for layer in range(L):
        for which in range(3):
            own(layer, which).start()

    def each_chunk(body, size=CHUNK):
        def step(index, _):
            body(pl.ds(pl.multiple_of(index * size, size), size))
            return 0

        lax.fori_loop(0, rows // size, step, 0)

    def put_stat(slot, where, left, right):
        lane = lax.broadcasted_iota(jnp.int32, (left.shape[0], 128), 1)
        wide = jnp.where(lane == 0, left, right)
        STAT[slot, t, :, where] = wide.T[:8]

    def stat_copy(slot, peer):
        return pltpu.make_async_remote_copy(
            STAT.at[slot, t], STAT.at[slot, t], ss.at[slot, peer], sr.at[slot, t],
            device_id={"tp": peer}, device_id_type=MESH,
        )

    def stat_arrival(slot, peer):
        return pltpu.make_async_remote_copy(
            STAT.at[slot, peer], STAT.at[slot, peer], ss.at[slot, peer], sr.at[slot, peer],
            device_id={"tp": peer}, device_id_type=MESH,
        )

    def send_stat(slot):
        for shift in range(1, T):
            stat_copy(slot, lax.rem(t + shift, T)).start()

    def wait_stat(slot):
        for shift in range(1, T):
            stat_arrival(slot, lax.rem(t + shift, T)).wait_recv()

    def total_stat(stat, where):
        total = stat[0, :, where]
        for peer in range(1, T):
            total = total + stat[peer, :, where]
        return jnp.concatenate([total] * 16, axis=0).T

    def part_ref(item, owner, half):
        layer, which, piece, pieces = table[item]
        slots = sources[which][1]
        size = slots.shape[2] // (2 * pieces)
        start = pl.multiple_of(half * (size * pieces) + piece * size, size)
        return slots.at[layer, owner, pl.ds(start, size)]

    def zcopy(item, owner, way):
        ref = part_ref(item, owner, g)
        sems = zs_right if way > 0 else zs_left
        return pltpu.make_async_remote_copy(
            ref, ref, sems.at[item, owner], zr.at[item, owner],
            device_id={"sp": me + way}, device_id_type=MESH,
        )

    def dcopy(item, owner):
        ref = part_ref(item, owner, 1 - g)
        return pltpu.make_async_remote_copy(
            ref, ref, ds.at[item], dr.at[item], device_id={"sp": me + inward}, device_id_type=MESH,
        )

    def ycopy(item, owner):
        ref = part_ref(item, owner, g)
        return pltpu.make_async_remote_copy(
            ref, ref, ys.at[item, owner], yr.at[item, owner],
            device_id={"grp": 1 - g}, device_id_type=MESH,
        )

    def yarrival(item, owner):
        ref = part_ref(item, owner, 1 - g)
        return pltpu.make_async_remote_copy(
            ref, ref, ys.at[item, owner], yr.at[item, owner],
            device_id={"grp": 1 - g}, device_id_type=MESH,
        )

    def outgoing(way):
        return low if way < 0 else high

    def send_out(ids):
        for item in ids:
            for way in (1, -1):

                @pl.when(outgoing(way))
                def _(item=item, way=way):
                    zcopy(item, me, way).start()

    def send_own(ids):
        for item in ids:
            for way in (1, -1):
                allowed = inside(item, me + way)
                if not folded(item):
                    allowed = both(allowed, no(outgoing(way)))

                @pl.when(allowed)
                def _(item=item, way=way):
                    zcopy(item, me, way).start()

    def send_direct(ids):
        for item in ids:
            if direct(item):
                dcopy(item, me).start()

    def take(ids, k, select=None):
        for item in ids:
            for way in (1, -1):
                owner = me - way * k
                ok = both(both(owner >= 0, owner < S), inside(item, me))
                if select is not None:
                    ok = both(ok, select(owner))

                @pl.when(ok)
                def _(item=item, way=way, owner=owner):
                    zcopy(item, owner, way).wait_recv()

                    @pl.when(inside(item, me + way))
                    def _():
                        zcopy(item, owner, way).start()

                    @pl.when(no(skips_y(item, owner)))
                    def _():
                        ycopy(item, owner).start()

    def arrive(ids, owner):
        for item in ids:
            skip = skips_y(item, owner)

            @pl.when(no(skip))
            def _(item=item):
                yarrival(item, owner).wait_recv()

            @pl.when(skip)
            def _(item=item):
                dcopy(item, owner).wait_recv()

    def x_ref(slot, source):
        return XG.at[source] if slot == L else X.at[slot, source]

    def xcopy(slot, source, peer, sem):
        return pltpu.make_async_remote_copy(
            x_ref(slot, source), x_ref(slot, source), sem, xr.at[slot, source],
            device_id={"tp": peer}, device_id_type=MESH,
        )

    def make_x(layer):
        source = h_ref if layer == 0 else HB

        def body(where):
            wide = source[where, :].astype(F32)
            X[layer, t, where, :] = (wide * gain_ref[layer : layer + 1, :]).astype(BF16)
            squares = jnp.sum(wide * wide, axis=1, keepdims=True)
            put_stat(2 * layer, where, squares, squares)

        each_chunk(body)

    def send_x(slot):
        for shift in range(1, chips):
            peer = lax.rem(chip + shift, chips) * 2 + core
            xcopy(slot, t, peer, xs.at[slot, shift]).start()
        xcopy(slot, t, partner, xs.at[slot, 0]).start()

    def relay_x(slot):
        for shift in range(1, chips):
            source = lax.rem(chip + shift, chips) * 2 + core
            xcopy(slot, source, partner, xf.at[slot, shift]).wait_recv()
            xcopy(slot, source, partner, xf.at[slot, shift]).start()

    def wait_x(slot):
        for shift in range(chips):
            source = lax.rem(chip + shift, chips) * 2 + 1 - core
            xcopy(slot, source, partner, xf.at[slot, 0]).wait_recv()

    def guest_x_copy():
        return pltpu.make_async_remote_copy(
            X.at[0, t], XG.at[t], xs.at[L, 0], xr.at[L, t],
            device_id={"sp": me + inward}, device_id_type=MESH,
        )

    def guest_stat_copy():
        return pltpu.make_async_remote_copy(
            STAT.at[0, t], GSTAT.at[t], gs.at[t], gr.at[t],
            device_id={"sp": me + inward}, device_id_type=MESH,
        )

    def guest_stat_pass(source, peer):
        return pltpu.make_async_remote_copy(
            GSTAT.at[source], GSTAT.at[source], gs.at[peer], gr.at[source],
            device_id={"tp": peer}, device_id_type=MESH,
        )

    def guest_back(index):
        start = pl.multiple_of(index * CHUNK + halo, 16)
        return pltpu.make_async_remote_copy(
            EXT.at[0, pl.ds(pl.multiple_of(guest_base + start, 16), CHUNK)],
            EXT.at[0, pl.ds(start, CHUNK)],
            bs.at[index], br.at[index],
            device_id={"sp": me + outward}, device_id_type=MESH,
        )

    def at_distance(k, body, select=None):
        if k == 0:
            body(me)
            return

        def step(index, _):
            owner = me + k - 2 * k * index
            ok = both(owner >= 0, owner < S)
            if select is not None:
                ok = both(ok, select(owner))

            @pl.when(ok)
            def _():
                body(owner)

            return 0

        lax.fori_loop(0, 2, step, 0)

    def multiply(total, x, layer, owner, start):
        at = lax.div(owner * Ds, Dt)
        columns = pl.ds(pl.multiple_of(lax.rem(owner * Ds, Dt), 128), Ds)
        xs_block = x[at, :, columns]
        for which, slots in ((0, WV), (1, WG)):
            part = jnp.dot(xs_block, slots[layer, owner], preferred_element_type=F32)
            if start:
                total[which] = part
            else:
                total[which] += part

    def project(layer, k, select=None):
        def block(owner):
            if k > 0:
                arrive(groups[layer][0] + groups[layer][1], owner)
            multiply(ACC, X.at[layer], layer, owner, k == 0)

        at_distance(k, block, select)

    def halo_copy(layer):
        end = halo + rows + (own_base if layer == 0 else 0)
        return pltpu.make_async_remote_copy(
            EXT.at[layer, pl.ds(pl.multiple_of(end - halo, 16), halo)],
            EXT.at[layer, pl.ds(0, halo)],
            hs.at[layer], hr.at[layer],
            device_id={"sp": me + 1}, device_id_type=MESH,
        )

    def sends_halo(layer):
        return both(no(last), no(first)) if layer == 0 else no(last)

    def takes_halo(layer):
        return both(no(first), no(low)) if layer == 0 else no(first)

    def gate_rows(layer, total, stat, base, where):
        mean = total_stat(stat, where)[:, :1] / features
        inv = lax.rsqrt(mean + epsilon)
        value, gating = total[0, where, :] * inv, total[1, where, :] * inv
        gated = (value / (1.0 + jnp.exp(-gating))).astype(BF16)
        EXT[layer, pl.ds(pl.multiple_of(base + where.start + halo, 16), where.size), :] = gated

    def gate(layer):
        base = own_base if layer == 0 else 0
        each_chunk(functools.partial(gate_rows, layer, ACC, STAT.at[2 * layer], base))

        @pl.when(sends_halo(layer))
        def _():
            halo_copy(layer).start()

    def convolve(layer):
        @pl.when(first)
        def _():
            EXT[layer, pl.ds(0, halo), :] = jnp.zeros((halo, Cn), BF16)

        @pl.when(takes_halo(layer))
        def _():
            halo_copy(layer).wait_recv()

        tall = CHUNK + halo + 8
        offset = halo - (taps - 1)
        base = own_base if layer == 0 else 0

        def body(where):
            if layer == 0:

                @pl.when(edge)
                def _():
                    guest_back(lax.div(where.start, CHUNK)).wait_recv()

            for column in range(0, Cn, 128):
                at = pl.ds(column, 128)
                window = EXT[layer, pl.ds(pl.multiple_of(base + where.start, 16), CHUNK + halo), at]
                tile = jnp.concatenate([window.astype(F32), jnp.zeros((8, 128), F32)], axis=0)
                total = jnp.zeros((CHUNK, 128), F32)
                for residue in range(8):
                    ks = [k for k in range(taps) if (k + offset) % 8 == residue]
                    if not ks:
                        continue
                    turned = pltpu.roll(tile, tall - residue, 0) if residue else tile
                    for k in ks:
                        low_row = k + offset - residue
                        total = total + taps_ref[layer, k : k + 1, at] * turned[low_row : low_row + CHUNK]
                CONV[where, at] = total
            conved = CONV[where, :]
            put_stat(
                2 * layer + 1, where,
                jnp.sum(conved, axis=1, keepdims=True),
                jnp.sum(conved * conved, axis=1, keepdims=True),
            )

        each_chunk(body)
        send_stat(2 * layer + 1)

    def mix(layer):
        wait_stat(2 * layer + 1)

        def body(where):
            stat = total_stat(STAT.at[2 * layer + 1], where)
            mean = stat[:, 0:1] / channels
            spread = stat[:, 1:2] / channels - mean * mean
            normed = (CONV[where, :] - mean) * lax.rsqrt(spread + epsilon) * ng_ref[
                layer : layer + 1, :
            ] + ns_ref[layer : layer + 1, :]
            MIX[where, :] = (normed / (1.0 + jnp.exp(-normed))).astype(BF16)

        each_chunk(body)

    def pair_copy(layer, at):
        return pltpu.make_async_remote_copy(
            PART.at[layer, 2 * at + 1 - core], PRECV.at[layer, at], ps.at[layer, at], pr.at[layer, at],
            device_id={"tp": partner}, device_id_type=MESH,
        )

    def sum_copy(layer, at):
        return pltpu.make_async_remote_copy(
            SUMB.at[layer, at], RECV.at[layer, chip], rs.at[layer, at], rr.at[layer, chip],
            device_id={"tp": at * 2 + core}, device_id_type=MESH,
        )

    def sum_arrival(layer, at):
        return pltpu.make_async_remote_copy(
            SUMB.at[layer, at], RECV.at[layer, at], rs.at[layer, at], rr.at[layer, at],
            device_id={"tp": at * 2 + core}, device_id_type=MESH,
        )

    def sum_pair(layer, at):
        pair_copy(layer, at).wait_recv()

        def body(where):
            SUMB[layer, at, where, :] = (
                PART[layer, at * 2 + core, where, :].astype(F32) + PRECV[layer, at, where, :].astype(F32)
            ).astype(BF16)

        each_chunk(body)
        sum_copy(layer, at).start()

    def branch(layer, k):
        def block(owner):
            if k > 0:
                arrive(groups[layer][2], owner)
            target = lax.div(owner * Ds, Dt)
            columns = pl.ds(pl.multiple_of(lax.rem(owner * Ds, Dt), 128), Ds)
            PART[layer, target, :, columns] = jnp.dot(
                MIX[...], WO[layer, owner], preferred_element_type=F32
            ).astype(BF16)
            if S == T:
                at = lax.div(target, 2)

                @pl.when(lax.rem(target, 2) != core)
                def _():
                    pair_copy(layer, at).start()

                @pl.when(both(lax.rem(target, 2) == core, at != chip))
                def _():
                    sum_pair(layer, at)

        at_distance(k, block)
        if S != T and k == S - 1:
            for shift in list(range(1, chips)) + [0]:
                pair_copy(layer, lax.rem(chip + shift, chips)).start()
            for shift in range(1, chips):
                sum_pair(layer, lax.rem(chip + shift, chips))

    def finish(layer):
        pair_copy(layer, chip).wait_recv()
        for shift in range(1, chips):
            sum_arrival(layer, lax.rem(chip + shift, chips)).wait_recv()
        source = h_ref if layer == 0 else HB
        target = out_ref if layer == L - 1 else HB

        def body(where):
            total = PART[layer, t, where, :].astype(F32) + PRECV[layer, chip, where, :].astype(F32)
            for shift in range(1, chips):
                total = total + RECV[layer, lax.rem(chip + shift, chips), where, :].astype(F32)
            target[where, :] = (source[where, :].astype(F32) + total).astype(BF16)

        each_chunk(body)

    barrier = pltpu.get_barrier_semaphore()
    for shift in range(1, T):
        pl.semaphore_signal(barrier, inc=1, device_id={"tp": lax.rem(t + shift, T)}, device_id_type=MESH)
    pl.semaphore_signal(barrier, inc=1, device_id={"grp": 1 - g}, device_id_type=MESH)

    @pl.when(no(first))
    def _():
        pl.semaphore_signal(barrier, inc=1, device_id={"sp": me - 1}, device_id_type=MESH)

    @pl.when(no(last))
    def _():
        pl.semaphore_signal(barrier, inc=1, device_id={"sp": me + 1}, device_id_type=MESH)

    inner = jnp.where(first, 0, 1) + jnp.where(last, 0, 1)
    pl.semaphore_wait(barrier, T + inner)

    value0, gating0, out0 = groups[0]
    later = [item for of_layer in groups[1:] for ids in of_layer for item in ids]
    for which in range(2):
        own(0, which).wait()
        send_own(groups[0][which])
    own(0, 2).wait()
    send_out(out0)
    for layer in range(1, L):
        for which in range(3):
            own(layer, which).wait()
            send_out(groups[layer][which])
    make_x(0)

    @pl.when(edge)
    def _():
        guest_x_copy().start()
        guest_stat_copy().start()
        send_direct(value0 + gating0)
        send_own(out0)
        send_direct(out0)
        for layer in range(1, L):
            send_own(groups[layer][0] + groups[layer][1])
            send_direct(groups[layer][0] + groups[layer][1])
            send_own(groups[layer][2])
        take(out0 + later, 1)

    def owned_inside(owner):
        return no(is_edge(owner))

    @pl.when(no(edge))
    def _():
        send_x(0)
        send_stat(0)
        take(value0 + gating0, 1)
        send_own(out0)
        relay_x(0)
        wait_x(0)
        project(0, 0)
        for k in range(2, S - 1):
            take(value0, k)
            if k == 2:

                @pl.when(near)
                def _():
                    xcopy(L, t, partner, xf.at[L, 0]).wait_recv()
                    guest_stat_pass(t, partner).wait_recv()
                    send_x(L)
                    for shift in range(1, T):
                        guest_stat_pass(t, lax.rem(t + shift, T)).start()

            take(gating0, k)
            project(0, k - 1, lambda owner: no(skips_y(value0[0], owner)))
        take(out0, 1, owned_inside)

        @pl.when(near)
        def _():
            relay_x(L)
            wait_x(L)
            for shift in range(1, T):
                guest_stat_pass(lax.rem(t + shift, T), partner).wait_recv()

        project(0, S - 2)
        wait_stat(0)

        @pl.when(near)
        def _():
            corner = jnp.where(low, 0, S - 1)
            arrive(value0 + gating0, corner)
            multiply(ACC, X.at[0], 0, corner, False)
            multiply(GACC, XG, 0, me, True)

            def add(index, _):
                owner = lax.rem(me + index, S)
                multiply(GACC, XG, 0, owner, False)
                return 0

            lax.fori_loop(1, S, add, 0)

            def back(where):
                gate_rows(0, GACC, GSTAT, guest_base, where)
                guest_back(lax.div(where.start, CHUNK)).start()

            each_chunk(back)

        gate(0)
        if L > 1:
            send_own(groups[1][0] + groups[1][1])

    for layer in range(L):
        value, gating, out = groups[layer]
        convolve(layer)
        if layer == 0:

            @pl.when(no(edge))
            def _():
                take(out0, 1, is_edge)

        else:

            @pl.when(no(edge))
            def _(out=out):
                take(out, 1)

        mix(layer)
        ahead = groups[layer + 1] if layer + 1 < L else None
        if ahead:

            @pl.when(no(edge))
            def _(ahead=ahead):
                take(ahead[0], 1)

        branch(layer, 0)
        take(out, 2)
        if ahead:

            @pl.when(no(edge))
            def _(ahead=ahead):
                take(ahead[1], 1)
                send_own(ahead[2])

        branch(layer, 1)
        for k in range(3, S):
            take(out, k)
            branch(layer, k - 1)
        branch(layer, S - 1)
        finish(layer)
        if ahead:
            make_x(layer + 1)
            send_x(layer + 1)
            send_stat(2 * layer + 2)
            take(ahead[0], 2)
            relay_x(layer + 1)
            take(ahead[1], 2)
            wait_x(layer + 1)
            project(layer + 1, 0)
            project(layer + 1, 1)
            for k in range(3, S):
                take(ahead[0] + ahead[1], k)
                project(layer + 1, k - 1)
            project(layer + 1, S - 1)
            wait_stat(2 * layer + 2)
            gate(layer + 1)

            @pl.when(edge)
            def _(ahead=ahead):
                send_direct(ahead[2])

            if layer + 2 < L:

                @pl.when(no(edge))
                def _(layer=layer):
                    send_own(groups[layer + 2][0] + groups[layer + 2][1])

    for item in range(items):

        def drain(owner, _, item=item):
            mine = owner == me
            had = either(mine, inside(item, me))

            @pl.when(both(both(owner <= me, inside(item, me + 1)), had))
            def _():
                zcopy(item, owner, 1).wait_send()

            @pl.when(both(both(owner >= me, inside(item, me - 1)), had))
            def _():
                zcopy(item, owner, -1).wait_send()

            @pl.when(both(no(mine), both(inside(item, me), no(skips_y(item, owner)))))
            def _():
                ycopy(item, owner).wait_send()

            return 0

        lax.fori_loop(0, S, drain, 0)
        if direct(item):

            @pl.when(edge)
            def _(item=item):
                dcopy(item, me).wait_send()

    def drain_x(slot):
        for shift in range(chips):
            xcopy(slot, t, partner, xs.at[slot, shift]).wait_send()
        for shift in range(1, chips):
            xcopy(slot, t, partner, xf.at[slot, shift]).wait_send()

    def drain_stat(slot):
        for shift in range(1, T):
            stat_copy(slot, lax.rem(t + shift, T)).wait_send()

    @pl.when(edge)
    def _():
        guest_x_copy().wait_send()
        guest_stat_copy().wait_send()

    @pl.when(no(edge))
    def _():
        drain_x(0)
        drain_stat(0)

    @pl.when(near)
    def _():
        drain_x(L)
        for shift in range(1, T):
            guest_stat_pass(t, lax.rem(t + shift, T)).wait_send()
        for index in range(rows // CHUNK):
            guest_back(index).wait_send()

    for layer in range(L):
        if layer > 0:
            drain_x(layer)
            drain_stat(2 * layer)
        drain_stat(2 * layer + 1)
        for shift in range(chips):
            pair_copy(layer, lax.rem(chip + shift, chips)).wait_send()
        for shift in range(1, chips):
            sum_copy(layer, lax.rem(chip + shift, chips)).wait_send()

        @pl.when(sends_halo(layer))
        def _(layer=layer):
            halo_copy(layer).wait_send()


def shards(hidden_in, in_gain, w_value, w_gate, conv_taps, norm_gain, norm_shift, w_out):
    S, T = lax.axis_size("sp"), lax.axis_size("tp")
    L, Ds, Cn = w_value.shape
    rows, Dt = hidden_in.shape
    chips = T // 2
    halo = (conv_taps.shape[1] - 1 + 15) // 16 * 16
    items = L * sum(PIECES)
    vmem = pl.BlockSpec(memory_space=pltpu.VMEM)
    hbm = pl.BlockSpec(memory_space=pl.ANY)
    dma = pltpu.SemaphoreType.DMA
    return pl.pallas_call(
        functools.partial(kernel, S, T),
        out_shape=jax.ShapeDtypeStruct((rows, Dt), BF16),
        in_specs=[vmem, vmem, hbm, hbm, vmem, vmem, vmem, hbm],
        out_specs=vmem,
        scratch_shapes=[
            pltpu.VMEM((L, S, Ds, Cn), BF16),
            pltpu.VMEM((L, S, Ds, Cn), BF16),
            pltpu.VMEM((L, S, Cn, Ds), BF16),
            pltpu.VMEM((L, T, rows, Dt), BF16),
            pltpu.VMEM((T, rows, Dt), BF16),
            pltpu.VMEM((2, rows, Cn), F32),
            pltpu.VMEM((2, rows, Cn), F32),
            pltpu.VMEM((L, halo + 2 * rows, Cn), BF16),
            pltpu.VMEM((rows, Cn), F32),
            pltpu.VMEM((rows, Cn), BF16),
            pltpu.VMEM((L, T, rows, Dt), BF16),
            pltpu.VMEM((L, chips, rows, Dt), BF16),
            pltpu.VMEM((L, chips, rows, Dt), BF16),
            pltpu.VMEM((L, chips, rows, Dt), BF16),
            pltpu.VMEM((2 * L, T, 8, rows), F32),
            pltpu.VMEM((T, 8, rows), F32),
            pltpu.VMEM((rows, Dt), BF16),
            dma((L, 3)),
            dma((items, S)), dma((items, S)), dma((items, S)), dma((items, S)), dma((items, S)),
            dma((items,)), dma((items,)),
            dma((L + 1, T)), dma((L + 1, chips)), dma((L + 1, chips)),
            dma((2 * L, T)), dma((2 * L, T)),
            dma((T,)), dma((T,)),
            dma((L,)), dma((L,)),
            dma((rows // CHUNK,)), dma((rows // CHUNK,)),
            dma((L, chips)), dma((L, chips)),
            dma((L, chips)), dma((L, chips)),
        ],
        compiler_params=pltpu.CompilerParams(
            collective_id=0, has_side_effects=True, vmem_limit_bytes=64_000_000
        ),
    )(hidden_in, in_gain, w_value, w_gate, conv_taps, norm_gain, norm_shift, w_out)


def solution(mesh):
    placed = (
        P(("grp", "sp"), "tp"),
        P(None, "tp"),
        P(None, "sp", "tp"),
        P(None, "sp", "tp"),
        P(None, None, "tp"),
        P(None, "tp"),
        P(None, "tp"),
        P(None, "tp", "sp"),
    )
    return jax.shard_map(
        shards, mesh=mesh, in_specs=placed, out_specs=P(("grp", "sp"), "tp"), check_vma=False
    )
```

time: 247 us -> 249 us (level)
    pallas_call x1, Pallas kernels: 243 us -> 245 us  [shards(): pl.pallas_call(functools.partial(kernel, S, T), out_shape=jax.ShapeDtypeS...]
where the time goes in v1:
time: 249 us
  Pallas kernels  245 us (98%)
  local copies, waits for them, and re-layouts  3.65 us (1%)
    pallas_call x1, Pallas kernels, shards(): pl.pallas_call(functools.partial(kernel, S, T), out_shape=jax.ShapeDtypeS...  245 us

profile of v1, /device:TPU:3, one launch (start us, length us, event | category | flops | bytes accessed | tf_op | source)
XLA Modules:
  0.0 249.1 jit_solution(6045207077671545896)
XLA Ops:
  0.0 1.6 copy.9.taps_ref
  1.6 245.4 %shard_map.82 = bf16[384,1024]{1,0:T(8,128)(2,1)} custom-call(bf16[384,1024]{1,0:T(8,128)(2,1)} %h_ref.1, f32[2,1024]{1,0:T(2,128)} %gain_ref.1, bf16[2,1024,512]{2,1,0:T(8,128)(2,1)} %wv_ref.1, bf16[2,1024,512]{2,1,0:T(8,128)(2,1)} %wg_ref.1, f32[2,31,512]{2,1,0:T(8,128)} %copy.9.taps_ref, f32[2,512]{1,0:T(2,128)} %ng_ref.1, f32[2,512]{1,0:T(2,128)} %ns_ref.1, ...), custom_call_target="tpu_custom_call" | custom-call | tf_op jit(solution)/shard_map/pallas_call | solution.py:728
  247.0 2.1 copy.11

commit v2 on v1

--- a/solution.py
+++ b/solution.py
@@ -9,8 +9,11 @@
 
 epsilon = 1e-06
 CHUNK = 128
-PIECES = (1, 1, 2)
 F32, BF16 = jnp.float32, jnp.bfloat16
+
+
+def cuts(Ds):
+    return (2, 2, 2) if Ds >= 512 else (1, 1, 1)
 
 
 def kernel(
@@ -25,6 +28,8 @@
     taps = taps_ref.shape[1]
     features, channels = Dt * T, Cn * T
     chips = T // 2
+    pieces_of = cuts(Ds)
+    Q, Dq = WO.shape[2], WO.shape[4]
     halo = EXT.shape[1] - 2 * rows
     g, me, t = lax.axis_index("grp"), lax.axis_index("sp"), lax.axis_index("tp")
     core = lax.rem(t, 2)
@@ -49,16 +54,16 @@
         of_layer = []
         for which in range(3):
             ids = []
-            for piece in range(PIECES[which]):
+            for piece in range(pieces_of[which]):
                 ids.append(len(table))
-                table.append((layer, which, piece, PIECES[which]))
+                table.append((layer, which, piece, pieces_of[which]))
             of_layer.append(ids)
         groups.append(of_layer)
     items = len(table)
 
     def direct(item):
-        layer, which, _, _ = table[item]
-        return (layer, which) != (0, 2)
+        layer, which, piece, _ = table[item]
+        return (layer, which) != (0, 1) or piece == 0
 
     def folded(item):
         layer, which, _, _ = table[item]
@@ -77,11 +82,23 @@
 
     def own(layer, which):
         source, slots = sources[which]
-        return pltpu.make_async_copy(source.at[layer], slots.at[layer, me], own_sem.at[layer, which])
+        if which < 2:
+            return [pltpu.make_async_copy(source.at[layer], slots.at[layer, me], own_sem.at[layer, which])]
+        return [
+            pltpu.make_async_copy(
+                source.at[layer, :, pl.ds(q * Dq, Dq)], slots.at[layer, me, q], own_sem.at[layer, 2 + q]
+            )
+            for q in range(Q)
+        ]
 
     for layer in range(L):
         for which in range(3):
-            own(layer, which).start()
+            for copy in own(layer, which):
+                copy.start()
+
+    def own_wait(layer, which):
+        for copy in own(layer, which):
+            copy.wait()
 
     def each_chunk(body, size=CHUNK):
         def step(index, _):
@@ -124,6 +141,8 @@
     def part_ref(item, owner, half):
         layer, which, piece, pieces = table[item]
         slots = sources[which][1]
+        if which == 2:
+            return slots.at[layer, owner, half * pieces + piece]
         size = slots.shape[2] // (2 * pieces)
         start = pl.multiple_of(half * (size * pieces) + piece * size, size)
         return slots.at[layer, owner, pl.ds(start, size)]
@@ -405,76 +424,115 @@
 
         each_chunk(body)
 
-    def pair_copy(layer, at):
-        return pltpu.make_async_remote_copy(
-            PART.at[layer, 2 * at + 1 - core], PRECV.at[layer, at], ps.at[layer, at], pr.at[layer, at],
-            device_id={"tp": partner}, device_id_type=MESH,
-        )
-
-    def sum_copy(layer, at):
-        return pltpu.make_async_remote_copy(
-            SUMB.at[layer, at], RECV.at[layer, chip], rs.at[layer, at], rr.at[layer, chip],
+    fine = Q if S == T else 1
+    width = Dt // fine
+
+    def cut(ref, q):
+        return ref if fine == 1 else ref.at[:, pl.ds(pl.multiple_of(q * width, 128), width)]
+
+    def pair_copy(layer, at, q):
+        return pltpu.make_async_remote_copy(
+            cut(PART.at[layer, 2 * at + 1 - core], q), cut(PRECV.at[layer, at], q),
+            ps.at[layer, at, q], pr.at[layer, at, q], device_id={"tp": partner}, device_id_type=MESH,
+        )
+
+    def sum_copy(layer, at, q):
+        return pltpu.make_async_remote_copy(
+            cut(SUMB.at[layer, at], q), cut(RECV.at[layer, chip], q),
+            rs.at[layer, at, q], rr.at[layer, chip, q],
             device_id={"tp": at * 2 + core}, device_id_type=MESH,
         )
 
-    def sum_arrival(layer, at):
-        return pltpu.make_async_remote_copy(
-            SUMB.at[layer, at], RECV.at[layer, at], rs.at[layer, at], rr.at[layer, at],
+    def sum_arrival(layer, at, q):
+        return pltpu.make_async_remote_copy(
+            cut(SUMB.at[layer, at], q), cut(RECV.at[layer, at], q),
+            rs.at[layer, at, q], rr.at[layer, at, q],
             device_id={"tp": at * 2 + core}, device_id_type=MESH,
         )
 
-    def sum_pair(layer, at):
-        pair_copy(layer, at).wait_recv()
+    def columns_of(q):
+        return pl.ds(pl.multiple_of(q * width, 128), width)
+
+    def sum_pair(layer, at, q):
+        pair_copy(layer, at, q).wait_recv()
+        columns = columns_of(q)
 
         def body(where):
-            SUMB[layer, at, where, :] = (
-                PART[layer, at * 2 + core, where, :].astype(F32) + PRECV[layer, at, where, :].astype(F32)
+            SUMB[layer, at, where, columns] = (
+                PART[layer, at * 2 + core, where, columns].astype(F32)
+                + PRECV[layer, at, where, columns].astype(F32)
             ).astype(BF16)
 
         each_chunk(body)
-        sum_copy(layer, at).start()
-
-    def branch(layer, k):
+        sum_copy(layer, at, q).start()
+
+    def turn_order():
+        count = Q // 2
+        return [(False, g * count + piece, piece) for piece in range(count)] + [
+            (True, (1 - g) * count + piece, piece) for piece in range(count)
+        ]
+
+    def branch(layer, k, select=None):
         def block(owner):
+            target = lax.div(owner * Ds, Dt)
+            base = lax.rem(owner * Ds, Dt)
+            at = lax.div(target, 2)
+
+            def product(q):
+                columns = pl.ds(pl.multiple_of(base + q * Dq, 128), Dq)
+                PART[layer, target, :, columns] = jnp.dot(
+                    MIX[...], WO[layer, owner, q], preferred_element_type=F32
+                ).astype(BF16)
+                if S == T:
+
+                    @pl.when(lax.rem(target, 2) != core)
+                    def _():
+                        pair_copy(layer, at, q).start()
+
+            def total(q):
+                if S == T:
+
+                    @pl.when(both(lax.rem(target, 2) == core, at != chip))
+                    def _():
+                        sum_pair(layer, at, q)
+
+            order = turn_order()
+            early = order if k == 0 else [o for o in order if not o[0]]
+            for _, q, _ in early:
+                product(q)
+            for _, q, _ in early:
+                total(q)
             if k > 0:
-                arrive(groups[layer][2], owner)
-            target = lax.div(owner * Ds, Dt)
-            columns = pl.ds(pl.multiple_of(lax.rem(owner * Ds, Dt), 128), Ds)
-            PART[layer, target, :, columns] = jnp.dot(
-                MIX[...], WO[layer, owner], preferred_element_type=F32
-            ).astype(BF16)
-            if S == T:
-                at = lax.div(target, 2)
-
-                @pl.when(lax.rem(target, 2) != core)
-                def _():
-                    pair_copy(layer, at).start()
-
-                @pl.when(both(lax.rem(target, 2) == core, at != chip))
-                def _():
-                    sum_pair(layer, at)
-
-        at_distance(k, block)
+                for _, q, piece in order[len(early) :]:
+                    arrive([groups[layer][2][piece]], owner)
+                    product(q)
+                    total(q)
+
+        at_distance(k, block, select)
         if S != T and k == S - 1:
             for shift in list(range(1, chips)) + [0]:
-                pair_copy(layer, lax.rem(chip + shift, chips)).start()
+                pair_copy(layer, lax.rem(chip + shift, chips), 0).start()
             for shift in range(1, chips):
-                sum_pair(layer, lax.rem(chip + shift, chips))
+                sum_pair(layer, lax.rem(chip + shift, chips), 0)
 
     def finish(layer):
-        pair_copy(layer, chip).wait_recv()
-        for shift in range(1, chips):
-            sum_arrival(layer, lax.rem(chip + shift, chips)).wait_recv()
         source = h_ref if layer == 0 else HB
         target = out_ref if layer == L - 1 else HB
-
-        def body(where):
-            total = PART[layer, t, where, :].astype(F32) + PRECV[layer, chip, where, :].astype(F32)
+        for q in [q for _, q, _ in turn_order()] if fine > 1 else [0]:
+            pair_copy(layer, chip, q).wait_recv()
             for shift in range(1, chips):
-                total = total + RECV[layer, lax.rem(chip + shift, chips), where, :].astype(F32)
-            target[where, :] = (source[where, :].astype(F32) + total).astype(BF16)
-
-        each_chunk(body)
+                sum_arrival(layer, lax.rem(chip + shift, chips), q).wait_recv()
+            columns = columns_of(q)
+
+            def body(where, columns=columns):
+                total = PART[layer, t, where, columns].astype(F32) + PRECV[
+                    layer, chip, where, columns
+                ].astype(F32)
+                for shift in range(1, chips):
+                    total = total + RECV[layer, lax.rem(chip + shift, chips), where, columns].astype(F32)
+                target[where, columns] = (source[where, columns].astype(F32) + total).astype(BF16)
+
+            each_chunk(body)
 
     barrier = pltpu.get_barrier_semaphore()
     for shift in range(1, T):
@@ -493,17 +551,24 @@
     pl.semaphore_wait(barrier, T + inner)
 
     value0, gating0, out0 = groups[0]
-    later = [item for of_layer in groups[1:] for ids in of_layer for item in ids]
     for which in range(2):
-        own(0, which).wait()
+        own_wait(0, which)
         send_own(groups[0][which])
-    own(0, 2).wait()
+    own_wait(0, 2)
     send_out(out0)
     for layer in range(1, L):
         for which in range(3):
-            own(layer, which).wait()
+            own_wait(layer, which)
             send_out(groups[layer][which])
     make_x(0)
+
+    def owned_inside(owner):
+        return no(is_edge(owner))
+
+    def inner_take(ids, k, select=None):
+        @pl.when(no(edge))
+        def _():
+            take(ids, k, select)
 
     @pl.when(edge)
     def _():
@@ -516,10 +581,12 @@
             send_own(groups[layer][0] + groups[layer][1])
             send_direct(groups[layer][0] + groups[layer][1])
             send_own(groups[layer][2])
-        take(out0 + later, 1)
-
-    def owned_inside(owner):
-        return no(is_edge(owner))
+            send_direct(groups[layer][2])
+        take(out0, 1)
+        for layer in range(1, L):
+            for which in range(3):
+                take(groups[layer][which], 1)
+        take(out0, 2)
 
     @pl.when(no(edge))
     def _():
@@ -577,73 +644,62 @@
             each_chunk(back)
 
         gate(0)
+        take(out0, 1, is_edge)
         if L > 1:
             send_own(groups[1][0] + groups[1][1])
+        take(out0, 2)
 
     for layer in range(L):
         value, gating, out = groups[layer]
+        ahead = groups[layer + 1] if layer + 1 < L else None
         convolve(layer)
-        if layer == 0:
-
-            @pl.when(no(edge))
-            def _():
-                take(out0, 1, is_edge)
-
-        else:
-
-            @pl.when(no(edge))
-            def _(out=out):
-                take(out, 1)
-
         mix(layer)
-        ahead = groups[layer + 1] if layer + 1 < L else None
+        branch(layer, 0)
         if ahead:
+            inner_take(ahead[0], 1, owned_inside)
+        branch(layer, 1)
+        branch(layer, 2)
+        for k in range(3, S):
+            take(out, k)
+            branch(layer, k)
+        if ahead:
+            inner_take(ahead[0], 1, is_edge)
+            inner_take(ahead[1], 1, owned_inside)
+        finish(layer)
+        if ahead:
+            after = layer + 1
+            make_x(after)
+            send_x(after)
+            send_stat(2 * after)
+            take(ahead[0], 2)
+            inner_take(ahead[1], 1, is_edge)
+            relay_x(after)
+            take(ahead[1], 2)
 
             @pl.when(no(edge))
             def _(ahead=ahead):
-                take(ahead[0], 1)
-
-        branch(layer, 0)
-        take(out, 2)
-        if ahead:
-
-            @pl.when(no(edge))
-            def _(ahead=ahead):
-                take(ahead[1], 1)
                 send_own(ahead[2])
 
-        branch(layer, 1)
-        for k in range(3, S):
-            take(out, k)
-            branch(layer, k - 1)
-        branch(layer, S - 1)
-        finish(layer)
-        if ahead:
-            make_x(layer + 1)
-            send_x(layer + 1)
-            send_stat(2 * layer + 2)
-            take(ahead[0], 2)
-            relay_x(layer + 1)
-            take(ahead[1], 2)
-            wait_x(layer + 1)
-            project(layer + 1, 0)
-            project(layer + 1, 1)
+            wait_x(after)
+            project(after, 0)
             for k in range(3, S):
-                take(ahead[0] + ahead[1], k)
-                project(layer + 1, k - 1)
-            project(layer + 1, S - 1)
-            wait_stat(2 * layer + 2)
-            gate(layer + 1)
-
-            @pl.when(edge)
-            def _(ahead=ahead):
-                send_direct(ahead[2])
-
-            if layer + 2 < L:
+                take(ahead[0], k)
+            inner_take(ahead[2], 1, owned_inside)
+            project(after, 1)
+            for k in range(3, S):
+                take(ahead[1], k)
+            for k in range(2, S):
+                project(after, k)
+            wait_stat(2 * after)
+            gate(after)
+            inner_take(ahead[2], 1, is_edge)
+            if after + 1 < L:
 
                 @pl.when(no(edge))
-                def _(layer=layer):
-                    send_own(groups[layer + 2][0] + groups[layer + 2][1])
+                def _(after=after):
+                    send_own(groups[after + 1][0] + groups[after + 1][1])
+
+            take(ahead[2], 2)
 
     for item in range(items):
 
@@ -706,9 +762,11 @@
             drain_stat(2 * layer)
         drain_stat(2 * layer + 1)
         for shift in range(chips):
-            pair_copy(layer, lax.rem(chip + shift, chips)).wait_send()
+            for q in range(fine):
+                pair_copy(layer, lax.rem(chip + shift, chips), q).wait_send()
         for shift in range(1, chips):
-            sum_copy(layer, lax.rem(chip + shift, chips)).wait_send()
+            for q in range(fine):
+                sum_copy(layer, lax.rem(chip + shift, chips), q).wait_send()
 
         @pl.when(sends_halo(layer))
         def _(layer=layer):
@@ -721,7 +779,9 @@
     rows, Dt = hidden_in.shape
     chips = T // 2
     halo = (conv_taps.shape[1] - 1 + 15) // 16 * 16
-    items = L * sum(PIECES)
+    items = L * sum(cuts(Ds))
+    Q = 2 * cuts(Ds)[2]
+    fine = Q if S == T else 1
     vmem = pl.BlockSpec(memory_space=pltpu.VMEM)
     hbm = pl.BlockSpec(memory_space=pl.ANY)
     dma = pltpu.SemaphoreType.DMA
@@ -733,7 +793,7 @@
         scratch_shapes=[
             pltpu.VMEM((L, S, Ds, Cn), BF16),
             pltpu.VMEM((L, S, Ds, Cn), BF16),
-            pltpu.VMEM((L, S, Cn, Ds), BF16),
+            pltpu.VMEM((L, S, Q, Cn, Ds // Q), BF16),
             pltpu.VMEM((L, T, rows, Dt), BF16),
             pltpu.VMEM((T, rows, Dt), BF16),
             pltpu.VMEM((2, rows, Cn), F32),
@@ -748,7 +808,7 @@
             pltpu.VMEM((2 * L, T, 8, rows), F32),
             pltpu.VMEM((T, 8, rows), F32),
             pltpu.VMEM((rows, Dt), BF16),
-            dma((L, 3)),
+            dma((L, 2 + Q)),
             dma((items, S)), dma((items, S)), dma((items, S)), dma((items, S)), dma((items, S)),
             dma((items,)), dma((items,)),
             dma((L + 1, T)), dma((L + 1, chips)), dma((L + 1, chips)),
@@ -756,8 +816,8 @@
             dma((T,)), dma((T,)),
             dma((L,)), dma((L,)),
             dma((rows // CHUNK,)), dma((rows // CHUNK,)),
-            dma((L, chips)), dma((L, chips)),
-            dma((L, chips)), dma((L, chips)),
+            dma((L, chips, fine)), dma((L, chips, fine)),
+            dma((L, chips, fine)), dma((L, chips, fine)),
         ],
         compiler_params=pltpu.CompilerParams(
             collective_id=0, has_side_effects=True, vmem_limit_bytes=64_000_000

time: 249 us -> 203 us (0.82)
  Pallas kernels: 245 us -> 198 us
    pallas_call x1, Pallas kernels: 245 us -> 198 us  [shards(): pl.pallas_call(functools.partial(kernel, S, T), out_shape=jax.ShapeDtypeS...]
where the time goes in v2:
time: 203 us; the launch traced here: 202 us
  Pallas kernels  198 us (98%)
  local copies, waits for them, and re-layouts  3.65 us (2%)
    pallas_call x1, Pallas kernels, shards(): pl.pallas_call(functools.partial(kernel, S, T), out_shape=jax.ShapeDtypeS...  198 us

profile of v2, /device:TPU:3, one launch (start us, length us, event | category | flops | bytes accessed | tf_op | source)
XLA Modules:
  0.0 201.6 jit_solution(14047135682896997935)
XLA Ops:
  0.0 1.6 copy.9.taps_ref
  1.6 198.0 %shard_map.82 = bf16[384,1024]{1,0:T(8,128)(2,1)} custom-call(bf16[384,1024]{1,0:T(8,128)(2,1)} %h_ref.1, f32[2,1024]{1,0:T(2,128)} %gain_ref.1, bf16[2,1024,512]{2,1,0:T(8,128)(2,1)} %wv_ref.1, bf16[2,1024,512]{2,1,0:T(8,128)(2,1)} %wg_ref.1, f32[2,31,512]{2,1,0:T(8,128)} %copy.9.taps_ref, f32[2,512]{1,0:T(2,128)} %ng_ref.1, f32[2,512]{1,0:T(2,128)} %ns_ref.1, ...), custom_call_target="tpu_custom_call" | custom-call | tf_op jit(solution)/shard_map/pallas_call | solution.py:788
  199.6 2.1 %copy.11 = bf16[384,1024]{1,0:T(8,128)(2,1)} copy(bf16[384,1024]{1,0:T(8,128)(2,1)} %shard_map.82) | data formatting | bytes 1572864

commit v3 on v2

--- a/solution.py
+++ b/solution.py
@@ -62,8 +62,8 @@
     items = len(table)
 
     def direct(item):
-        layer, which, piece, _ = table[item]
-        return (layer, which) != (0, 1) or piece == 0
+        _, which, piece, _ = table[item]
+        return which != 1 or piece == 0
 
     def folded(item):
         layer, which, _, _ = table[item]
@@ -91,10 +91,12 @@
             for q in range(Q)
         ]
 
-    for layer in range(L):
-        for which in range(3):
-            for copy in own(layer, which):
-                copy.start()
+    def own_start(layer, which):
+        for copy in own(layer, which):
+            copy.start()
+
+    own_start(0, 0)
+    own_start(0, 1)
 
     def own_wait(layer, which):
         for copy in own(layer, which):
@@ -554,12 +556,12 @@
     for which in range(2):
         own_wait(0, which)
         send_own(groups[0][which])
-    own_wait(0, 2)
-    send_out(out0)
-    for layer in range(1, L):
-        for which in range(3):
-            own_wait(layer, which)
-            send_out(groups[layer][which])
+    rest = [(0, 2)] + [(layer, which) for layer in range(1, L) for which in range(3)]
+    for layer, which in rest:
+        own_start(layer, which)
+    for layer, which in rest:
+        own_wait(layer, which)
+        send_out(groups[layer][which])
     make_x(0)
 
     def owned_inside(owner):
@@ -569,6 +571,15 @@
         @pl.when(no(edge))
         def _():
             take(ids, k, select)
+
+    def edge_take(ids, k):
+        @pl.when(edge)
+        def _():
+            take(ids, k)
+
+    def far_take(ids):
+        for k in range(3, S):
+            take(ids, k)
 
     @pl.when(edge)
     def _():
@@ -587,6 +598,8 @@
             for which in range(3):
                 take(groups[layer][which], 1)
         take(out0, 2)
+        if L > 1:
+            take(groups[1][0][:1], 2)
 
     @pl.when(no(edge))
     def _():
@@ -610,6 +623,8 @@
                         guest_stat_pass(t, lax.rem(t + shift, T)).start()
 
             take(gating0, k)
+            if k == 2 and L > 1:
+                send_own(groups[1][0])
             project(0, k - 1, lambda owner: no(skips_y(value0[0], owner)))
         take(out0, 1, owned_inside)
 
@@ -620,6 +635,8 @@
             for shift in range(1, T):
                 guest_stat_pass(lax.rem(t + shift, T), partner).wait_recv()
 
+        if L > 1:
+            take(groups[1][0][:1], 1, owned_inside)
         project(0, S - 2)
         wait_stat(0)
 
@@ -646,60 +663,75 @@
         gate(0)
         take(out0, 1, is_edge)
         if L > 1:
-            send_own(groups[1][0] + groups[1][1])
-        take(out0, 2)
+            send_own(groups[1][1])
+            take(groups[1][0][1:], 1, owned_inside)
 
     for layer in range(L):
-        value, gating, out = groups[layer]
+        out = groups[layer][2]
         ahead = groups[layer + 1] if layer + 1 < L else None
+        if ahead and layer > 0:
+            inner_take(ahead[0], 1, owned_inside)
+            edge_take(ahead[0][:1], 2)
         convolve(layer)
+        inner_take(out[1:] if layer > 0 else out[:1], 2)
+        if layer > 0:
+            far_take(out[:1])
         mix(layer)
+        if layer == 0:
+            inner_take(out[1:], 2)
+        if ahead:
+            edge_take(ahead[0][1:], 2)
         branch(layer, 0)
+        branch(layer, 1)
         if ahead:
-            inner_take(ahead[0], 1, owned_inside)
-        branch(layer, 1)
+            inner_take(ahead[1][:1], 1, owned_inside)
         branch(layer, 2)
-        for k in range(3, S):
-            take(out, k)
-            branch(layer, k)
+        far_take(out[1:] if layer > 0 else out)
         if ahead:
             inner_take(ahead[0], 1, is_edge)
-            inner_take(ahead[1], 1, owned_inside)
+            inner_take(ahead[1][1:], 1, owned_inside)
+            edge_take(ahead[1][:1], 2)
+        for k in range(3, S):
+            branch(layer, k)
         finish(layer)
         if ahead:
             after = layer + 1
             make_x(after)
             send_x(after)
             send_stat(2 * after)
-            take(ahead[0], 2)
+            inner_take(ahead[0], 2)
             inner_take(ahead[1], 1, is_edge)
-            relay_x(after)
-            take(ahead[1], 2)
 
             @pl.when(no(edge))
             def _(ahead=ahead):
                 send_own(ahead[2])
 
+            edge_take(ahead[1][1:], 2)
+            far_take(ahead[0])
+            inner_take(ahead[1], 2)
+            relay_x(after)
+            far_take(ahead[1][:1])
             wait_x(after)
             project(after, 0)
+            project(after, 1)
+            inner_take(ahead[2][:1], 1, owned_inside)
+            far_take(ahead[1][1:])
+            project(after, 2)
+            inner_take(ahead[2][1:], 1, owned_inside)
+            edge_take(ahead[2][:1], 2)
             for k in range(3, S):
-                take(ahead[0], k)
-            inner_take(ahead[2], 1, owned_inside)
-            project(after, 1)
-            for k in range(3, S):
-                take(ahead[1], k)
-            for k in range(2, S):
                 project(after, k)
             wait_stat(2 * after)
             gate(after)
             inner_take(ahead[2], 1, is_edge)
+            edge_take(ahead[2][1:], 2)
             if after + 1 < L:
 
                 @pl.when(no(edge))
                 def _(after=after):
                     send_own(groups[after + 1][0] + groups[after + 1][1])
 
-            take(ahead[2], 2)
+            inner_take(ahead[2][:1], 2)
 
     for item in range(items):
 

time: 203 us -> 193 us (0.951)
  Pallas kernels: 198 us -> 190 us
    pallas_call x1, Pallas kernels: 198 us -> 190 us  [shards(): pl.pallas_call(functools.partial(kernel, S, T), out_shape=jax.ShapeDtypeS...]
where the time goes in v3:
time: 193 us
  Pallas kernels  190 us (98%)
  local copies, waits for them, and re-layouts  3.65 us (2%)
    pallas_call x1, Pallas kernels, shards(): pl.pallas_call(functools.partial(kernel, S, T), out_shape=jax.ShapeDtypeS...  190 us

profile of v3, /device:TPU:3, one launch (start us, length us, event | category | flops | bytes accessed | tf_op | source)
XLA Modules:
  0.0 193.2 jit_solution(10929214219667928053)
XLA Ops:
  0.0 1.6 copy.9.taps_ref
  1.6 189.6 %shard_map.82 = bf16[384,1024]{1,0:T(8,128)(2,1)} custom-call(bf16[384,1024]{1,0:T(8,128)(2,1)} %h_ref.1, f32[2,1024]{1,0:T(2,128)} %gain_ref.1, bf16[2,1024,512]{2,1,0:T(8,128)(2,1)} %wv_ref.1, bf16[2,1024,512]{2,1,0:T(8,128)(2,1)} %wg_ref.1, f32[2,31,512]{2,1,0:T(8,128)} %copy.9.taps_ref, f32[2,512]{1,0:T(2,128)} %ng_ref.1, f32[2,512]{1,0:T(2,128)} %ns_ref.1, ...), custom_call_target="tpu_custom_call" | custom-call | tf_op jit(solution)/shard_map/pallas_call | solution.py:820
  191.2 2.1 %copy.11 = bf16[384,1024]{1,0:T(8,128)(2,1)} copy(bf16[384,1024]{1,0:T(8,128)(2,1)} %shard_map.82) | data formatting | bytes 1572864

commit v4 on v3

--- a/solution.py
+++ b/solution.py
@@ -19,13 +19,13 @@
 def kernel(
     S, T, h_ref, gain_ref, wv_ref, wg_ref, taps_ref, ng_ref, ns_ref, wo_ref, out_ref,
     WV, WG, WO, X, XG, ACC, GACC, EXT, CONV, MIX, PART, PRECV, SUMB, RECV, STAT, GSTAT, HB,
-    own_sem, zr, zs_right, zs_left, yr, ys, dr, ds, xr, xs, xf, sr, ss, gr, gs, hr, hs, br, bs,
+    own_sem, zr, zs, zo, yr, ys, xr, xs, xf, sr, ss, gr, gs, hr, hs, br, bs,
     pr, ps, rr, rs,
 ):
     L = wv_ref.shape[0]
     Ds, Cn = wv_ref.shape[1], wv_ref.shape[2]
     rows, Dt = h_ref.shape
-    taps = taps_ref.shape[1]
+    taps = taps_ref.shape[0]
     features, channels = Dt * T, Cn * T
     chips = T // 2
     pieces_of = cuts(Ds)
@@ -86,7 +86,7 @@
             return [pltpu.make_async_copy(source.at[layer], slots.at[layer, me], own_sem.at[layer, which])]
         return [
             pltpu.make_async_copy(
-                source.at[layer, :, pl.ds(q * Dq, Dq)], slots.at[layer, me, q], own_sem.at[layer, 2 + q]
+                source.at[layer, :, pl.ds(q * Dq, Dq)], slots.at[layer, me, q], own_sem.at[layer, 2]
             )
             for q in range(Q)
         ]
@@ -99,8 +99,8 @@
     own_start(0, 1)
 
     def own_wait(layer, which):
-        for copy in own(layer, which):
-            copy.wait()
+        slot = sources[which][1].at[layer, me]
+        pltpu.make_async_copy(slot, slot, own_sem.at[layer, which]).wait()
 
     def each_chunk(body, size=CHUNK):
         def step(index, _):
@@ -116,13 +116,13 @@
 
     def stat_copy(slot, peer):
         return pltpu.make_async_remote_copy(
-            STAT.at[slot, t], STAT.at[slot, t], ss.at[slot, peer], sr.at[slot, t],
+            STAT.at[slot, t], STAT.at[slot, t], ss.at[slot], sr.at[slot, t],
             device_id={"tp": peer}, device_id_type=MESH,
         )
 
     def stat_arrival(slot, peer):
         return pltpu.make_async_remote_copy(
-            STAT.at[slot, peer], STAT.at[slot, peer], ss.at[slot, peer], sr.at[slot, peer],
+            STAT.at[slot, peer], STAT.at[slot, peer], ss.at[slot], sr.at[slot, peer],
             device_id={"tp": peer}, device_id_type=MESH,
         )
 
@@ -151,29 +151,39 @@
 
     def zcopy(item, owner, way):
         ref = part_ref(item, owner, g)
-        sems = zs_right if way > 0 else zs_left
-        return pltpu.make_async_remote_copy(
-            ref, ref, sems.at[item, owner], zr.at[item, owner],
+        layer, which, _, _ = table[item]
+        return pltpu.make_async_remote_copy(
+            ref, ref, zs.at[layer, which, owner], zr.at[item, owner],
+            device_id={"sp": me + way}, device_id_type=MESH,
+        )
+
+    def zown(item, way):
+        ref = part_ref(item, me, g)
+        layer, which, _, _ = table[item]
+        return pltpu.make_async_remote_copy(
+            ref, ref, zo.at[layer, which, (way + 1) // 2], zr.at[item, me],
             device_id={"sp": me + way}, device_id_type=MESH,
         )
 
     def dcopy(item, owner):
         ref = part_ref(item, owner, 1 - g)
-        return pltpu.make_async_remote_copy(
-            ref, ref, ds.at[item], dr.at[item], device_id={"sp": me + inward}, device_id_type=MESH,
+        layer, which, _, _ = table[item]
+        return pltpu.make_async_remote_copy(
+            ref, ref, ys.at[layer, which, owner], yr.at[item, owner],
+            device_id={"sp": me + inward}, device_id_type=MESH,
         )
 
     def ycopy(item, owner):
         ref = part_ref(item, owner, g)
         return pltpu.make_async_remote_copy(
-            ref, ref, ys.at[item, owner], yr.at[item, owner],
+            ref, ref, ys.at[table[item][0], table[item][1], owner], yr.at[item, owner],
             device_id={"grp": 1 - g}, device_id_type=MESH,
         )
 
     def yarrival(item, owner):
         ref = part_ref(item, owner, 1 - g)
         return pltpu.make_async_remote_copy(
-            ref, ref, ys.at[item, owner], yr.at[item, owner],
+            ref, ref, ys.at[table[item][0], table[item][1], owner], yr.at[item, owner],
             device_id={"grp": 1 - g}, device_id_type=MESH,
         )
 
@@ -186,7 +196,7 @@
 
                 @pl.when(outgoing(way))
                 def _(item=item, way=way):
-                    zcopy(item, me, way).start()
+                    zown(item, way).start()
 
     def send_own(ids):
         for item in ids:
@@ -197,7 +207,7 @@
 
                 @pl.when(allowed)
                 def _(item=item, way=way):
-                    zcopy(item, me, way).start()
+                    zown(item, way).start()
 
     def send_direct(ids):
         for item in ids:
@@ -226,15 +236,7 @@
 
     def arrive(ids, owner):
         for item in ids:
-            skip = skips_y(item, owner)
-
-            @pl.when(no(skip))
-            def _(item=item):
-                yarrival(item, owner).wait_recv()
-
-            @pl.when(skip)
-            def _(item=item):
-                dcopy(item, owner).wait_recv()
+            yarrival(item, owner).wait_recv()
 
     def x_ref(slot, source):
         return XG.at[source] if slot == L else X.at[slot, source]
@@ -281,13 +283,13 @@
 
     def guest_stat_copy():
         return pltpu.make_async_remote_copy(
-            STAT.at[0, t], GSTAT.at[t], gs.at[t], gr.at[t],
+            STAT.at[0, t], GSTAT.at[t], gs.at[0], gr.at[t],
             device_id={"sp": me + inward}, device_id_type=MESH,
         )
 
     def guest_stat_pass(source, peer):
         return pltpu.make_async_remote_copy(
-            GSTAT.at[source], GSTAT.at[source], gs.at[peer], gr.at[source],
+            GSTAT.at[source], GSTAT.at[source], gs.at[0], gr.at[source],
             device_id={"tp": peer}, device_id_type=MESH,
         )
 
@@ -400,7 +402,7 @@
                     turned = pltpu.roll(tile, tall - residue, 0) if residue else tile
                     for k in ks:
                         low_row = k + offset - residue
-                        total = total + taps_ref[layer, k : k + 1, at] * turned[low_row : low_row + CHUNK]
+                        total = total + taps_ref[k, layer : layer + 1, at] * turned[low_row : low_row + CHUNK]
                 CONV[where, at] = total
             conved = CONV[where, :]
             put_stat(
@@ -435,20 +437,20 @@
     def pair_copy(layer, at, q):
         return pltpu.make_async_remote_copy(
             cut(PART.at[layer, 2 * at + 1 - core], q), cut(PRECV.at[layer, at], q),
-            ps.at[layer, at, q], pr.at[layer, at, q], device_id={"tp": partner}, device_id_type=MESH,
+            ps.at[layer, at], pr.at[layer, at, q], device_id={"tp": partner}, device_id_type=MESH,
         )
 
     def sum_copy(layer, at, q):
         return pltpu.make_async_remote_copy(
             cut(SUMB.at[layer, at], q), cut(RECV.at[layer, chip], q),
-            rs.at[layer, at, q], rr.at[layer, chip, q],
+            rs.at[layer, at], rr.at[layer, chip, q],
             device_id={"tp": at * 2 + core}, device_id_type=MESH,
         )
 
     def sum_arrival(layer, at, q):
         return pltpu.make_async_remote_copy(
             cut(SUMB.at[layer, at], q), cut(RECV.at[layer, at], q),
-            rs.at[layer, at, q], rr.at[layer, at, q],
+            rs.at[layer, at], rr.at[layer, at, q],
             device_id={"tp": at * 2 + core}, device_id_type=MESH,
         )
 
@@ -474,7 +476,7 @@
             (True, (1 - g) * count + piece, piece) for piece in range(count)
         ]
 
-    def branch(layer, k, select=None):
+    def branch(layer, k, part=None):
         def block(owner):
             target = lax.div(owner * Ds, Dt)
             base = lax.rem(owner * Ds, Dt)
@@ -500,18 +502,19 @@
 
             order = turn_order()
             early = order if k == 0 else [o for o in order if not o[0]]
-            for _, q, _ in early:
-                product(q)
-            for _, q, _ in early:
-                total(q)
-            if k > 0:
+            if part != 1:
+                for _, q, _ in early:
+                    product(q)
+                for _, q, _ in early:
+                    total(q)
+            if k > 0 and part != 0:
                 for _, q, piece in order[len(early) :]:
                     arrive([groups[layer][2][piece]], owner)
                     product(q)
                     total(q)
 
-        at_distance(k, block, select)
-        if S != T and k == S - 1:
+        at_distance(k, block)
+        if S != T and k == S - 1 and part != 0:
             for shift in list(range(1, chips)) + [0]:
                 pair_copy(layer, lax.rem(chip + shift, chips), 0).start()
             for shift in range(1, chips):
@@ -535,6 +538,98 @@
                 target[where, columns] = (source[where, columns].astype(F32) + total).astype(BF16)
 
             each_chunk(body)
+
+    def sent(ref, sem):
+        pltpu.make_async_remote_copy(
+            ref, ref, sem, zr.at[0, 0], device_id={"tp": partner}, device_id_type=MESH
+        ).wait_send()
+
+    def half_ref(layer, which, owner, half):
+        slots = sources[which][1]
+        size = slots.shape[2] // 2
+        return slots.at[layer, owner, pl.ds(pl.multiple_of(half * size, size), size)]
+
+    def drain(layer, which):
+        ids = groups[layer][which]
+        whole = [item for item in ids if direct(item)]
+        for way in (1, -1):
+
+            @pl.when(inside(ids[0], me + way))
+            def _(way=way):
+                sent(half_ref(layer, which, me, g), zo.at[layer, which, (way + 1) // 2])
+
+        @pl.when(edge)
+        def _():
+            if len(whole) == len(ids):
+                sent(half_ref(layer, which, me, 1 - g), ys.at[layer, which, me])
+            else:
+                for item in whole:
+                    sent(part_ref(item, me, 1 - g), ys.at[layer, which, me])
+
+        def settle(owner, _):
+            @pl.when(both(owner != me, inside(ids[0], me)))
+            def _():
+                @pl.when(inside(ids[0], jnp.where(owner < me, me + 1, me - 1)))
+                def _():
+                    sent(half_ref(layer, which, owner, g), zs.at[layer, which, owner])
+
+                skip = skips_y(whole[0], owner)
+
+                @pl.when(no(skip))
+                def _():
+                    sent(half_ref(layer, which, owner, g), ys.at[layer, which, owner])
+
+                if len(whole) < len(ids):
+
+                    @pl.when(skip)
+                    def _():
+                        for item in ids:
+                            if item not in whole:
+                                sent(part_ref(item, owner, g), ys.at[layer, which, owner])
+
+            return 0
+
+        lax.fori_loop(0, S, settle, 0)
+
+    def drain_x(slot):
+        for shift in range(chips):
+            xcopy(slot, t, partner, xs.at[slot, shift]).wait_send()
+        for shift in range(1, chips):
+            xcopy(slot, t, partner, xf.at[slot, shift]).wait_send()
+
+    def drain_stat(slot):
+        sent(STAT.at[slot, pl.ds(0, T - 1)], ss.at[slot])
+
+    def drain_start():
+        @pl.when(edge)
+        def _():
+            guest_x_copy().wait_send()
+            guest_stat_copy().wait_send()
+
+        @pl.when(no(edge))
+        def _():
+            drain_x(0)
+            drain_stat(0)
+
+        @pl.when(near)
+        def _():
+            drain_x(L)
+            sent(GSTAT.at[pl.ds(0, T - 1)], gs.at[0])
+            for index in range(rows // CHUNK):
+                guest_back(index).wait_send()
+
+    def drain_sums(layer):
+        for shift in range(chips):
+            at = lax.rem(chip + shift, chips)
+            sent(PRECV.at[layer, at], ps.at[layer, at])
+        for shift in range(1, chips):
+            at = lax.rem(chip + shift, chips)
+            sent(SUMB.at[layer, at], rs.at[layer, at])
+
+    def drain_halo(layer):
+        @pl.when(sends_halo(layer))
+        def _():
+            halo_copy(layer).wait_send()
 
     barrier = pltpu.get_barrier_semaphore()
     for shift in range(1, T):
@@ -637,6 +732,7 @@
 
         if L > 1:
             take(groups[1][0][:1], 1, owned_inside)
+        take(out0[:1], 1, is_edge)
         project(0, S - 2)
         wait_stat(0)
 
@@ -661,7 +757,7 @@
             each_chunk(back)
 
         gate(0)
-        take(out0, 1, is_edge)
+        take(out0[1:], 1, is_edge)
         if L > 1:
             send_own(groups[1][1])
             take(groups[1][0][1:], 1, owned_inside)
@@ -686,21 +782,34 @@
         if ahead:
             inner_take(ahead[1][:1], 1, owned_inside)
         branch(layer, 2)
+        if ahead is None:
+            drain_stat(2 * layer + 1)
+            drain_halo(layer)
+            if layer > 0:
+                drain_x(layer)
+                drain_stat(2 * layer)
+                drain(layer, 0)
+                drain(layer, 1)
         far_take(out[1:] if layer > 0 else out)
+        for k in range(3, S):
+            branch(layer, k, 0)
         if ahead:
             inner_take(ahead[0], 1, is_edge)
             inner_take(ahead[1][1:], 1, owned_inside)
             edge_take(ahead[1][:1], 2)
         for k in range(3, S):
-            branch(layer, k)
+            branch(layer, k, 1)
+        if ahead:
+            inner_take(ahead[1][:1], 1, is_edge)
+            inner_take(ahead[0][:1], 2)
+            inner_take(ahead[1][1:], 1, is_edge)
         finish(layer)
         if ahead:
             after = layer + 1
             make_x(after)
             send_x(after)
             send_stat(2 * after)
-            inner_take(ahead[0], 2)
-            inner_take(ahead[1], 1, is_edge)
+            inner_take(ahead[0][1:], 2)
 
             @pl.when(no(edge))
             def _(ahead=ahead):
@@ -709,21 +818,34 @@
             edge_take(ahead[1][1:], 2)
             far_take(ahead[0])
             inner_take(ahead[1], 2)
+            if layer == 0:
+                drain_start()
+                drain(0, 0)
+                drain(0, 1)
             relay_x(after)
             far_take(ahead[1][:1])
+            drain_stat(2 * layer + 1)
+            drain_halo(layer)
+            drain_sums(layer)
+            far_take(ahead[1][1:])
             wait_x(after)
             project(after, 0)
             project(after, 1)
             inner_take(ahead[2][:1], 1, owned_inside)
-            far_take(ahead[1][1:])
+            drain(layer, 2)
+            if layer > 0:
+                drain_x(layer)
+                drain_stat(2 * layer)
+                drain(layer, 0)
+                drain(layer, 1)
+            inner_take(ahead[2][1:], 1, owned_inside)
+            inner_take(ahead[2], 1, is_edge)
             project(after, 2)
-            inner_take(ahead[2][1:], 1, owned_inside)
             edge_take(ahead[2][:1], 2)
             for k in range(3, S):
                 project(after, k)
             wait_stat(2 * after)
             gate(after)
-            inner_take(ahead[2], 1, is_edge)
             edge_take(ahead[2][1:], 2)
             if after + 1 < L:
 
@@ -733,76 +855,8 @@
 
             inner_take(ahead[2][:1], 2)
 
-    for item in range(items):
-
-        def drain(owner, _, item=item):
-            mine = owner == me
-            had = either(mine, inside(item, me))
-
-            @pl.when(both(both(owner <= me, inside(item, me + 1)), had))
-            def _():
-                zcopy(item, owner, 1).wait_send()
-
-            @pl.when(both(both(owner >= me, inside(item, me - 1)), had))
-            def _():
-                zcopy(item, owner, -1).wait_send()
-
-            @pl.when(both(no(mine), both(inside(item, me), no(skips_y(item, owner)))))
-            def _():
-                ycopy(item, owner).wait_send()
-
-            return 0
-
-        lax.fori_loop(0, S, drain, 0)
-        if direct(item):
-
-            @pl.when(edge)
-            def _(item=item):
-                dcopy(item, me).wait_send()
-
-    def drain_x(slot):
-        for shift in range(chips):
-            xcopy(slot, t, partner, xs.at[slot, shift]).wait_send()
-        for shift in range(1, chips):
-            xcopy(slot, t, partner, xf.at[slot, shift]).wait_send()
-
-    def drain_stat(slot):
-        for shift in range(1, T):
-            stat_copy(slot, lax.rem(t + shift, T)).wait_send()
-
-    @pl.when(edge)
-    def _():
-        guest_x_copy().wait_send()
-        guest_stat_copy().wait_send()
-
-    @pl.when(no(edge))
-    def _():
-        drain_x(0)
-        drain_stat(0)
-
-    @pl.when(near)
-    def _():
-        drain_x(L)
-        for shift in range(1, T):
-            guest_stat_pass(t, lax.rem(t + shift, T)).wait_send()
-        for index in range(rows // CHUNK):
-            guest_back(index).wait_send()
-
-    for layer in range(L):
-        if layer > 0:
-            drain_x(layer)
-            drain_stat(2 * layer)
-        drain_stat(2 * layer + 1)
-        for shift in range(chips):
-            for q in range(fine):
-                pair_copy(layer, lax.rem(chip + shift, chips), q).wait_send()
-        for shift in range(1, chips):
-            for q in range(fine):
-                sum_copy(layer, lax.rem(chip + shift, chips), q).wait_send()
-
-        @pl.when(sends_halo(layer))
-        def _(layer=layer):
-            halo_copy(layer).wait_send()
+    drain(L - 1, 2)
+    drain_sums(L - 1)
 
 
 def shards(hidden_in, in_gain, w_value, w_gate, conv_taps, norm_gain, norm_shift, w_out):
@@ -840,21 +894,20 @@
             pltpu.VMEM((2 * L, T, 8, rows), F32),
             pltpu.VMEM((T, 8, rows), F32),
             pltpu.VMEM((rows, Dt), BF16),
-            dma((L, 2 + Q)),
-            dma((items, S)), dma((items, S)), dma((items, S)), dma((items, S)), dma((items, S)),
-            dma((items,)), dma((items,)),
+            dma((L, 3)),
+            dma((items, S)), dma((L, 3, S)), dma((L, 3, 2)), dma((items, S)), dma((L, 3, S)),
             dma((L + 1, T)), dma((L + 1, chips)), dma((L + 1, chips)),
-            dma((2 * L, T)), dma((2 * L, T)),
-            dma((T,)), dma((T,)),
+            dma((2 * L, T)), dma((2 * L,)),
+            dma((T,)), dma((1,)),
             dma((L,)), dma((L,)),
             dma((rows // CHUNK,)), dma((rows // CHUNK,)),
-            dma((L, chips, fine)), dma((L, chips, fine)),
-            dma((L, chips, fine)), dma((L, chips, fine)),
+            dma((L, chips, fine)), dma((L, chips)),
+            dma((L, chips, fine)), dma((L, chips)),
         ],
         compiler_params=pltpu.CompilerParams(
             collective_id=0, has_side_effects=True, vmem_limit_bytes=64_000_000
         ),
-    )(hidden_in, in_gain, w_value, w_gate, conv_taps, norm_gain, norm_shift, w_out)
+    )(hidden_in, in_gain, w_value, w_gate, jnp.swapaxes(conv_taps, 0, 1), norm_gain, norm_shift, w_out)
 
 
 def solution(mesh):

time: 193 us -> 184 us (0.953)
  Pallas kernels: 190 us -> 181 us
    pallas_call x1, Pallas kernels: 190 us -> 181 us  [shards(): pl.pallas_call(functools.partial(kernel, S, T), out_shape=jax.ShapeDtypeS...]
where the time goes in v4:
time: 184 us; the launch traced here: 183 us
  Pallas kernels  181 us (98%)
  local copies, waits for them, and re-layouts  2.06 us (1%)
    pallas_call x1, Pallas kernels, shards(): pl.pallas_call(functools.partial(kernel, S, T), out_shape=jax.ShapeDtypeS...  181 us

profile of v4, /device:TPU:3, one launch (start us, length us, event | category | flops | bytes accessed | tf_op | source)
XLA Modules:
  0.0 183.0 jit_solution(6626662060644532191)
XLA Ops:
  0.0 180.9 %shard_map.82 = bf16[384,1024]{1,0:T(8,128)(2,1)} custom-call(bf16[384,1024]{1,0:T(8,128)(2,1)} %h_ref.1, f32[2,1024]{1,0:T(2,128)} %gain_ref.1, bf16[2,1024,512]{2,1,0:T(8,128)(2,1)} %wv_ref.1, bf16[2,1024,512]{2,1,0:T(8,128)(2,1)} %wg_ref.1, f32[31,2,512]{2,1,0:T(2,128)} %bitcast.1, f32[2,512]{1,0:T(2,128)} %ng_ref.1, f32[2,512]{1,0:T(2,128)} %ns_ref.1, ...), custom_call_target="tpu_custom_call" | custom-call | tf_op jit(solution)/shard_map/pallas_call | solution.py:874
  180.9 2.1 %copy.10 = bf16[384,1024]{1,0:T(8,128)(2,1)} copy(bf16[384,1024]{1,0:T(8,128)(2,1)} %shard_map.82) | data formatting | bytes 1572864

commit v5 on v4

--- a/solution.py
+++ b/solution.py
@@ -12,8 +12,10 @@
 F32, BF16 = jnp.float32, jnp.bfloat16
 
 
-def cuts(Ds):
-    return (2, 2, 2) if Ds >= 512 else (1, 1, 1)
+def cuts(Ds, layer):
+    if Ds < 512:
+        return (1, 1, 1)
+    return (2, 2, 2) if layer == 0 else (2, 4, 4)
 
 
 def kernel(
@@ -28,7 +30,6 @@
     taps = taps_ref.shape[0]
     features, channels = Dt * T, Cn * T
     chips = T // 2
-    pieces_of = cuts(Ds)
     Q, Dq = WO.shape[2], WO.shape[4]
     halo = EXT.shape[1] - 2 * rows
     g, me, t = lax.axis_index("grp"), lax.axis_index("sp"), lax.axis_index("tp")
@@ -54,16 +55,22 @@
         of_layer = []
         for which in range(3):
             ids = []
-            for piece in range(pieces_of[which]):
+            for piece in range(cuts(Ds, layer)[which]):
                 ids.append(len(table))
-                table.append((layer, which, piece, pieces_of[which]))
+                table.append((layer, which, piece, cuts(Ds, layer)[which]))
             of_layer.append(ids)
         groups.append(of_layer)
     items = len(table)
 
+    def fore(ids):
+        return ids[: (len(ids) + 1) // 2]
+
+    def aft(ids):
+        return ids[(len(ids) + 1) // 2 :]
+
     def direct(item):
-        _, which, piece, _ = table[item]
-        return which != 1 or piece == 0
+        _, which, piece, pieces = table[item]
+        return which != 1 or 2 * piece < pieces
 
     def folded(item):
         layer, which, _, _ = table[item]
@@ -102,37 +109,51 @@
         slot = sources[which][1].at[layer, me]
         pltpu.make_async_copy(slot, slot, own_sem.at[layer, which]).wait()
 
-    def each_chunk(body, size=CHUNK):
+    def each_chunk(body, start=0, count=rows):
         def step(index, _):
-            body(pl.ds(pl.multiple_of(index * size, size), size))
+            body(pl.ds(pl.multiple_of(index * CHUNK, CHUNK), CHUNK))
             return 0
 
-        lax.fori_loop(0, rows // size, step, 0)
+        lax.fori_loop(start // CHUNK, (start + count) // CHUNK, step, 0)
+
+    def parts_of(layer):
+        return [(0, rows)]
 
     def put_stat(slot, where, left, right):
         lane = lax.broadcasted_iota(jnp.int32, (left.shape[0], 128), 1)
         wide = jnp.where(lane == 0, left, right)
         STAT[slot, t, :, where] = wide.T[:8]
 
-    def stat_copy(slot, peer):
-        return pltpu.make_async_remote_copy(
-            STAT.at[slot, t], STAT.at[slot, t], ss.at[slot], sr.at[slot, t],
+    def stat_ref(slot, source, part):
+        if slot % 2 == 0:
+            return STAT.at[slot, source]
+        start, count = parts_of(slot // 2)[part]
+        return STAT.at[slot, source, :, pl.ds(start, count)]
+
+    def stat_sem(slot, part):
+        return 2 * L + slot // 2 if part else slot
+
+    def stat_copy(slot, peer, part):
+        at = stat_sem(slot, part)
+        return pltpu.make_async_remote_copy(
+            stat_ref(slot, t, part), stat_ref(slot, t, part), ss.at[at], sr.at[at, t],
             device_id={"tp": peer}, device_id_type=MESH,
         )
 
-    def stat_arrival(slot, peer):
-        return pltpu.make_async_remote_copy(
-            STAT.at[slot, peer], STAT.at[slot, peer], ss.at[slot], sr.at[slot, peer],
+    def stat_arrival(slot, peer, part):
+        at = stat_sem(slot, part)
+        return pltpu.make_async_remote_copy(
+            stat_ref(slot, peer, part), stat_ref(slot, peer, part), ss.at[at], sr.at[at, peer],
             device_id={"tp": peer}, device_id_type=MESH,
         )
 
-    def send_stat(slot):
+    def send_stat(slot, part=0):
         for shift in range(1, T):
-            stat_copy(slot, lax.rem(t + shift, T)).start()
-
-    def wait_stat(slot):
+            stat_copy(slot, lax.rem(t + shift, T), part).start()
+
+    def wait_stat(slot, part=0):
         for shift in range(1, T):
-            stat_arrival(slot, lax.rem(t + shift, T)).wait_recv()
+            stat_arrival(slot, lax.rem(t + shift, T), part).wait_recv()
 
     def total_stat(stat, where):
         total = stat[0, :, where]
@@ -144,7 +165,9 @@
         layer, which, piece, pieces = table[item]
         slots = sources[which][1]
         if which == 2:
-            return slots.at[layer, owner, half * pieces + piece]
+            split = 2 * pieces // Q
+            size = Cn // split
+            return slots.at[layer, owner, half * (Q // 2) + piece // split, pl.ds(piece % split * size, size)]
         size = slots.shape[2] // (2 * pieces)
         start = pl.multiple_of(half * (size * pieces) + piece * size, size)
         return slots.at[layer, owner, pl.ds(start, size)]
@@ -304,7 +327,10 @@
 
     def at_distance(k, body, select=None):
         if k == 0:
-            body(me)
+            if select is None:
+                body(me)
+            else:
+                pl.when(select(me))(lambda: body(me))
             return
 
         def step(index, _):
@@ -370,14 +396,17 @@
         def _():
             halo_copy(layer).start()
 
-    def convolve(layer):
-        @pl.when(first)
-        def _():
-            EXT[layer, pl.ds(0, halo), :] = jnp.zeros((halo, Cn), BF16)
-
-        @pl.when(takes_halo(layer))
-        def _():
-            halo_copy(layer).wait_recv()
+    def convolve(layer, part):
+        start, count = parts_of(layer)[part]
+        if start == 0:
+
+            @pl.when(first)
+            def _():
+                EXT[layer, pl.ds(0, halo), :] = jnp.zeros((halo, Cn), BF16)
+
+            @pl.when(takes_halo(layer))
+            def _():
+                halo_copy(layer).wait_recv()
 
         tall = CHUNK + halo + 8
         offset = halo - (taps - 1)
@@ -411,11 +440,12 @@
                 jnp.sum(conved * conved, axis=1, keepdims=True),
             )
 
-        each_chunk(body)
-        send_stat(2 * layer + 1)
-
-    def mix(layer):
-        wait_stat(2 * layer + 1)
+        each_chunk(body, start, count)
+        send_stat(2 * layer + 1, part)
+
+    def mix(layer, part):
+        start, count = parts_of(layer)[part]
+        wait_stat(2 * layer + 1, part)
 
         def body(where):
             stat = total_stat(STAT.at[2 * layer + 1], where)
@@ -426,39 +456,41 @@
             ] + ns_ref[layer : layer + 1, :]
             MIX[where, :] = (normed / (1.0 + jnp.exp(-normed))).astype(BF16)
 
-        each_chunk(body)
+        each_chunk(body, start, count)
 
     fine = Q if S == T else 1
     width = Dt // fine
 
-    def cut(ref, q):
-        return ref if fine == 1 else ref.at[:, pl.ds(pl.multiple_of(q * width, 128), width)]
-
-    def pair_copy(layer, at, q):
-        return pltpu.make_async_remote_copy(
-            cut(PART.at[layer, 2 * at + 1 - core], q), cut(PRECV.at[layer, at], q),
-            ps.at[layer, at], pr.at[layer, at, q], device_id={"tp": partner}, device_id_type=MESH,
-        )
-
-    def sum_copy(layer, at, q):
-        return pltpu.make_async_remote_copy(
-            cut(SUMB.at[layer, at], q), cut(RECV.at[layer, chip], q),
-            rs.at[layer, at], rr.at[layer, chip, q],
+    def cut(layer, ref, q, part):
+        start, count = parts_of(layer)[part]
+        return ref.at[pl.ds(start, count), columns_of(q)]
+
+    def columns_of(q):
+        return pl.ds(0, width) if fine == 1 else pl.ds(pl.multiple_of(q * width, 128), width)
+
+    def pair_copy(layer, at, q, part):
+        return pltpu.make_async_remote_copy(
+            cut(layer, PART.at[layer, 2 * at + 1 - core], q, part), cut(layer, PRECV.at[layer, at], q, part),
+            ps.at[layer, at], pr.at[layer, at, part, q],
+            device_id={"tp": partner}, device_id_type=MESH,
+        )
+
+    def sum_copy(layer, at, q, part):
+        return pltpu.make_async_remote_copy(
+            cut(layer, SUMB.at[layer, at], q, part), cut(layer, RECV.at[layer, chip], q, part),
+            rs.at[layer, at], rr.at[layer, chip, part, q],
             device_id={"tp": at * 2 + core}, device_id_type=MESH,
         )
 
-    def sum_arrival(layer, at, q):
-        return pltpu.make_async_remote_copy(
-            cut(SUMB.at[layer, at], q), cut(RECV.at[layer, at], q),
-            rs.at[layer, at], rr.at[layer, at, q],
+    def sum_arrival(layer, at, q, part):
+        return pltpu.make_async_remote_copy(
+            cut(layer, SUMB.at[layer, at], q, part), cut(layer, RECV.at[layer, at], q, part),
+            rs.at[layer, at], rr.at[layer, at, part, q],
             device_id={"tp": at * 2 + core}, device_id_type=MESH,
         )
 
-    def columns_of(q):
-        return pl.ds(pl.multiple_of(q * width, 128), width)
-
-    def sum_pair(layer, at, q):
-        pair_copy(layer, at, q).wait_recv()
+    def sum_pair(layer, at, q, part):
+        pair_copy(layer, at, q, part).wait_recv()
         columns = columns_of(q)
 
         def body(where):
@@ -467,8 +499,8 @@
                 + PRECV[layer, at, where, columns].astype(F32)
             ).astype(BF16)
 
-        each_chunk(body)
-        sum_copy(layer, at, q).start()
+        each_chunk(body, *parts_of(layer)[part])
+        sum_copy(layer, at, q, part).start()
 
     def turn_order():
         count = Q // 2
@@ -476,68 +508,88 @@
             (True, (1 - g) * count + piece, piece) for piece in range(count)
         ]
 
-    def branch(layer, k, part=None):
+    def branch(layer, k, parts, early=True, late=True, wait=True, only=None, select=None, together=False):
         def block(owner):
             target = lax.div(owner * Ds, Dt)
             base = lax.rem(owner * Ds, Dt)
             at = lax.div(target, 2)
 
-            def product(q):
+            def product(q, part):
+                start, count = parts_of(layer)[part]
                 columns = pl.ds(pl.multiple_of(base + q * Dq, 128), Dq)
-                PART[layer, target, :, columns] = jnp.dot(
-                    MIX[...], WO[layer, owner, q], preferred_element_type=F32
+                PART[layer, target, pl.ds(start, count), columns] = jnp.dot(
+                    MIX[pl.ds(start, count), :], WO[layer, owner, q], preferred_element_type=F32
                 ).astype(BF16)
                 if S == T:
 
                     @pl.when(lax.rem(target, 2) != core)
                     def _():
-                        pair_copy(layer, at, q).start()
-
-            def total(q):
+                        pair_copy(layer, at, q, part).start()
+
+            def total(q, part):
                 if S == T:
 
                     @pl.when(both(lax.rem(target, 2) == core, at != chip))
                     def _():
-                        sum_pair(layer, at, q)
-
-            order = turn_order()
-            early = order if k == 0 else [o for o in order if not o[0]]
-            if part != 1:
-                for _, q, _ in early:
-                    product(q)
-                for _, q, _ in early:
-                    total(q)
-            if k > 0 and part != 0:
-                for _, q, piece in order[len(early) :]:
-                    arrive([groups[layer][2][piece]], owner)
-                    product(q)
-                    total(q)
-
-        at_distance(k, block)
-        if S != T and k == S - 1 and part != 0:
-            for shift in list(range(1, chips)) + [0]:
-                pair_copy(layer, lax.rem(chip + shift, chips), 0).start()
-            for shift in range(1, chips):
-                sum_pair(layer, lax.rem(chip + shift, chips), 0)
+                        sum_pair(layer, at, q, part)
+
+            order = [o for o in turn_order() if only is None or o[2] in only]
+            group = order if k == 0 or together else [o for o in order if not o[0]]
+            if together and k > 0:
+                arrive(groups[layer][2], owner)
+            if early:
+                for part in parts:
+                    for _, q, _ in group:
+                        product(q, part)
+                    for _, q, _ in group:
+                        total(q, part)
+            if k > 0 and late:
+                for _, q, piece in order[len(group) :]:
+                    if wait:
+                        ids = groups[layer][2]
+                        split = 2 * len(ids) // Q
+                        arrive(ids[piece * split : (piece + 1) * split], owner)
+                    for part in parts:
+                        product(q, part)
+                    for part in parts:
+                        total(q, part)
+
+        at_distance(k, block, select)
+
+    def stays(owner):
+        return lax.div(owner * Ds, 2 * Dt) == chip
+
+    def leaves(owner):
+        return no(stays(owner))
+
+    def share(layer):
+        if S != T:
+            for part in range(len(parts_of(layer))):
+                for shift in list(range(1, chips)) + [0]:
+                    pair_copy(layer, lax.rem(chip + shift, chips), 0, part).start()
+                for shift in range(1, chips):
+                    sum_pair(layer, lax.rem(chip + shift, chips), 0, part)
 
     def finish(layer):
+        share(layer)
         source = h_ref if layer == 0 else HB
         target = out_ref if layer == L - 1 else HB
-        for q in [q for _, q, _ in turn_order()] if fine > 1 else [0]:
-            pair_copy(layer, chip, q).wait_recv()
-            for shift in range(1, chips):
-                sum_arrival(layer, lax.rem(chip + shift, chips), q).wait_recv()
-            columns = columns_of(q)
-
-            def body(where, columns=columns):
-                total = PART[layer, t, where, columns].astype(F32) + PRECV[
-                    layer, chip, where, columns
-                ].astype(F32)
+        for part, (start, count) in enumerate(parts_of(layer)):
+            for q in [q for _, q, _ in turn_order()] if fine > 1 else [0]:
+                pair_copy(layer, chip, q, part).wait_recv()
                 for shift in range(1, chips):
-                    total = total + RECV[layer, lax.rem(chip + shift, chips), where, columns].astype(F32)
-                target[where, columns] = (source[where, columns].astype(F32) + total).astype(BF16)
-
-            each_chunk(body)
+                    sum_arrival(layer, lax.rem(chip + shift, chips), q, part).wait_recv()
+                columns = columns_of(q)
+
+                def body(where, columns=columns):
+                    total = PART[layer, t, where, columns].astype(F32) + PRECV[
+                        layer, chip, where, columns
+                    ].astype(F32)
+                    for shift in range(1, chips):
+                        total = total + RECV[layer, lax.rem(chip + shift, chips), where, columns].astype(F32)
+                    target[where, columns] = (source[where, columns].astype(F32) + total).astype(BF16)
+
+                each_chunk(body, start, count)
 
     def sent(ref, sem):
         pltpu.make_async_remote_copy(
@@ -549,6 +601,14 @@
         size = slots.shape[2] // 2
         return slots.at[layer, owner, pl.ds(pl.multiple_of(half * size, size), size)]
 
+    def some_ref(layer, which, owner, half, begin, count, pieces):
+        if count == pieces:
+            return half_ref(layer, which, owner, half)
+        slots = sources[which][1]
+        size = slots.shape[2] // (2 * pieces)
+        start = pl.multiple_of(half * (size * pieces) + begin * size, size)
+        return slots.at[layer, owner, pl.ds(start, size * count)]
+
     def drain(layer, which):
         ids = groups[layer][which]
         whole = [item for item in ids if direct(item)]
@@ -560,11 +620,7 @@
 
         @pl.when(edge)
         def _():
-            if len(whole) == len(ids):
-                sent(half_ref(layer, which, me, 1 - g), ys.at[layer, which, me])
-            else:
-                for item in whole:
-                    sent(part_ref(item, me, 1 - g), ys.at[layer, which, me])
+            sent(some_ref(layer, which, me, 1 - g, 0, len(whole), len(ids)), ys.at[layer, which, me])
 
         def settle(owner, _):
             @pl.when(both(owner != me, inside(ids[0], me)))
@@ -583,9 +639,10 @@
 
                     @pl.when(skip)
                     def _():
-                        for item in ids:
-                            if item not in whole:
-                                sent(part_ref(item, owner, g), ys.at[layer, which, owner])
+                        sent(
+                            some_ref(layer, which, owner, g, len(whole), len(ids) - len(whole), len(ids)),
+                            ys.at[layer, which, owner],
+                        )
 
             return 0
 
@@ -598,7 +655,11 @@
             xcopy(slot, t, partner, xf.at[slot, shift]).wait_send()
 
     def drain_stat(slot):
-        sent(STAT.at[slot, pl.ds(0, T - 1)], ss.at[slot])
+        if slot % 2 == 0:
+            sent(STAT.at[slot, pl.ds(0, T - 1)], ss.at[slot])
+            return
+        for part, (start, count) in enumerate(parts_of(slot // 2)):
+            sent(STAT.at[slot, pl.ds(0, T - 1), :, pl.ds(start, count)], ss.at[stat_sem(slot, part)])
 
     def drain_start():
         @pl.when(edge)
@@ -694,7 +755,7 @@
                 take(groups[layer][which], 1)
         take(out0, 2)
         if L > 1:
-            take(groups[1][0][:1], 2)
+            take(fore(groups[1][0]), 2)
 
     @pl.when(no(edge))
     def _():
@@ -731,8 +792,8 @@
                 guest_stat_pass(lax.rem(t + shift, T), partner).wait_recv()
 
         if L > 1:
-            take(groups[1][0][:1], 1, owned_inside)
-        take(out0[:1], 1, is_edge)
+            take(fore(groups[1][0]), 1, owned_inside)
+        take(fore(out0), 1, is_edge)
         project(0, S - 2)
         wait_stat(0)
 
@@ -757,31 +818,62 @@
             each_chunk(back)
 
         gate(0)
-        take(out0[1:], 1, is_edge)
+        take(aft(out0), 1, is_edge)
         if L > 1:
             send_own(groups[1][1])
-            take(groups[1][0][1:], 1, owned_inside)
+            take(aft(groups[1][0]), 1, owned_inside)
 
     for layer in range(L):
         out = groups[layer][2]
         ahead = groups[layer + 1] if layer + 1 < L else None
+        every = list(range(len(parts_of(layer))))
+        columns = list(range(Q // 2))
+        head_columns, tail_columns = columns[: Q // 4], columns[Q // 4 :]
         if ahead and layer > 0:
             inner_take(ahead[0], 1, owned_inside)
-            edge_take(ahead[0][:1], 2)
-        convolve(layer)
-        inner_take(out[1:] if layer > 0 else out[:1], 2)
-        if layer > 0:
-            far_take(out[:1])
-        mix(layer)
+            edge_take(fore(ahead[0]), 2)
         if layer == 0:
-            inner_take(out[1:], 2)
+            convolve(0, 0)
+            inner_take(fore(out), 2)
+            mix(0, 0)
+            inner_take(aft(out), 2)
+        else:
+            inner_take(aft(out), 2)
+            convolve(layer, 0)
+            far_take(fore(out))
+            mix(layer, 0)
+            for k in range(3):
+                branch(layer, k, every, select=leaves, together=True)
+            far_take(aft(out)[:1])
+            for k in range(3, S):
+                branch(layer, k, every, late=False, only=head_columns, select=leaves)
+            far_take(aft(out)[1:])
+            for k in range(3):
+                branch(layer, k, every, select=stays, together=True)
+            for k in range(3, S):
+                branch(layer, k, every, late=False, only=head_columns, select=stays)
         if ahead:
-            edge_take(ahead[0][1:], 2)
-        branch(layer, 0)
-        branch(layer, 1)
-        if ahead:
-            inner_take(ahead[1][:1], 1, owned_inside)
-        branch(layer, 2)
+            edge_take(aft(ahead[0]), 2)
+        if layer == 0:
+            branch(layer, 0, [0])
+            branch(layer, 1, [0])
+            far_take(fore(out))
+            if ahead:
+                inner_take(fore(ahead[1]), 1, owned_inside)
+                inner_take(fore(ahead[0]), 1, is_edge)
+            branch(layer, 2, [0], late=False)
+            if ahead:
+                inner_take(aft(ahead[0]), 1, is_edge)
+                inner_take(aft(ahead[1]), 1, owned_inside)
+            branch(layer, 2, [0], early=False)
+        else:
+            for k in range(3, S):
+                branch(layer, k, every, early=False, only=head_columns)
+                branch(layer, k, every, late=False, only=tail_columns)
+            if ahead:
+                inner_take(fore(ahead[1]), 1, owned_inside)
+                inner_take(ahead[0], 1, is_edge)
+                inner_take(aft(ahead[1]), 1, owned_inside)
         if ahead is None:
             drain_stat(2 * layer + 1)
             drain_halo(layer)
@@ -790,70 +882,89 @@
                 drain_stat(2 * layer)
                 drain(layer, 0)
                 drain(layer, 1)
-        far_take(out[1:] if layer > 0 else out)
-        for k in range(3, S):
-            branch(layer, k, 0)
+        if layer == 0:
+            far_take(aft(out))
+        for k in range(3, S) if layer == 0 else []:
+            branch(layer, k, every, late=False)
         if ahead:
-            inner_take(ahead[0], 1, is_edge)
-            inner_take(ahead[1][1:], 1, owned_inside)
-            edge_take(ahead[1][:1], 2)
-        for k in range(3, S):
-            branch(layer, k, 1)
+            edge_take(fore(ahead[1]), 2)
+            for k in range(3, S):
+                branch(layer, k, every, early=False, only=head_columns)
+            edge_take(aft(ahead[1])[:1], 2)
+            for k in range(3, S):
+                branch(layer, k, every, early=False, only=tail_columns)
+        else:
+            for k in range(3, S):
+                branch(layer, k, every, early=False, only=tail_columns)
         if ahead:
-            inner_take(ahead[1][:1], 1, is_edge)
-            inner_take(ahead[0][:1], 2)
-            inner_take(ahead[1][1:], 1, is_edge)
+            inner_take(fore(ahead[1]), 1, is_edge)
+            inner_take(fore(ahead[0]), 2)
+            inner_take(aft(ahead[1]), 1, is_edge)
+        last_share = lax.div(jnp.where(first, S - 1, 0) * Ds, Dt)
+        afar = both(edge, last_share == t)
+        if ahead:
+
+            @pl.when(afar)
+            def _(ahead=ahead):
+                take(aft(ahead[1])[1:], 2)
+                far_take(fore(ahead[0]))
+
         finish(layer)
         if ahead:
             after = layer + 1
             make_x(after)
             send_x(after)
             send_stat(2 * after)
-            inner_take(ahead[0][1:], 2)
+            inner_take(aft(ahead[0]), 2)
 
             @pl.when(no(edge))
             def _(ahead=ahead):
                 send_own(ahead[2])
 
-            edge_take(ahead[1][1:], 2)
-            far_take(ahead[0])
+
+            @pl.when(no(afar))
+            def _(ahead=ahead):
+                edge_take(aft(ahead[1])[1:], 2)
+                far_take(fore(ahead[0]))
+
+            far_take(aft(ahead[0]))
             inner_take(ahead[1], 2)
             if layer == 0:
                 drain_start()
                 drain(0, 0)
                 drain(0, 1)
+            far_take(ahead[1])
             relay_x(after)
-            far_take(ahead[1][:1])
             drain_stat(2 * layer + 1)
             drain_halo(layer)
             drain_sums(layer)
-            far_take(ahead[1][1:])
             wait_x(after)
             project(after, 0)
             project(after, 1)
-            inner_take(ahead[2][:1], 1, owned_inside)
+            inner_take(fore(ahead[2]), 1, owned_inside)
             drain(layer, 2)
             if layer > 0:
                 drain_x(layer)
                 drain_stat(2 * layer)
                 drain(layer, 0)
                 drain(layer, 1)
-            inner_take(ahead[2][1:], 1, owned_inside)
+            inner_take(aft(ahead[2]), 1, owned_inside)
             inner_take(ahead[2], 1, is_edge)
             project(after, 2)
-            edge_take(ahead[2][:1], 2)
+            edge_take(fore(ahead[2]), 2)
+            edge_take(aft(ahead[2])[:1], 2)
             for k in range(3, S):
                 project(after, k)
             wait_stat(2 * after)
             gate(after)
-            edge_take(ahead[2][1:], 2)
+            edge_take(aft(ahead[2])[1:], 2)
             if after + 1 < L:
 
                 @pl.when(no(edge))
                 def _(after=after):
                     send_own(groups[after + 1][0] + groups[after + 1][1])
 
-            inner_take(ahead[2][:1], 2)
+            inner_take(fore(ahead[2]), 2)
 
     drain(L - 1, 2)
     drain_sums(L - 1)
@@ -865,8 +976,8 @@
     rows, Dt = hidden_in.shape
     chips = T // 2
     halo = (conv_taps.shape[1] - 1 + 15) // 16 * 16
-    items = L * sum(cuts(Ds))
-    Q = 2 * cuts(Ds)[2]
+    items = sum(sum(cuts(Ds, layer)) for layer in range(L))
+    Q = 2 * cuts(Ds, 0)[2]
     fine = Q if S == T else 1
     vmem = pl.BlockSpec(memory_space=pltpu.VMEM)
     hbm = pl.BlockSpec(memory_space=pl.ANY)
@@ -901,8 +1012,8 @@
             dma((T,)), dma((1,)),
             dma((L,)), dma((L,)),
             dma((rows // CHUNK,)), dma((rows // CHUNK,)),
-            dma((L, chips, fine)), dma((L, chips)),
-            dma((L, chips, fine)), dma((L, chips)),
+            dma((L, chips, 1, fine)), dma((L, chips)),
+            dma((L, chips, 1, fine)), dma((L, chips)),
         ],
         compiler_params=pltpu.CompilerParams(
             collective_id=0, has_side_effects=True, vmem_limit_bytes=64_000_000

time: 184 us -> 183 us (level)
  no operation moved by 1% of the time
where the time goes in v5:
time: 183 us; the launch traced here: 182 us
  Pallas kernels  180 us (98%)
  local copies, waits for them, and re-layouts  2.06 us (1%)
    pallas_call x1, Pallas kernels, shards(): pl.pallas_call(functools.partial(kernel, S, T), out_shape=jax.ShapeDtypeS...  180 us

profile of v5, /device:TPU:3, one launch (start us, length us, event | category | flops | bytes accessed | tf_op | source)
XLA Modules:
  0.0 181.9 jit_solution(17997047843770630497)
XLA Ops:
  0.0 179.8 %shard_map.82 = bf16[384,1024]{1,0:T(8,128)(2,1)} custom-call(bf16[384,1024]{1,0:T(8,128)(2,1)} %h_ref.1, f32[2,1024]{1,0:T(2,128)} %gain_ref.1, bf16[2,1024,512]{2,1,0:T(8,128)(2,1)} %wv_ref.1, bf16[2,1024,512]{2,1,0:T(8,128)(2,1)} %wg_ref.1, f32[31,2,512]{2,1,0:T(2,128)} %bitcast.1, f32[2,512]{1,0:T(2,128)} %ng_ref.1, f32[2,512]{1,0:T(2,128)} %ns_ref.1, ...), custom_call_target="tpu_custom_call" | custom-call | tf_op jit(solution)/shard_map/pallas_call | solution.py:985
  179.8 2.1 %copy.10 = bf16[384,1024]{1,0:T(8,128)(2,1)} copy(bf16[384,1024]{1,0:T(8,128)(2,1)} %shard_map.82) | data formatting | bytes 1572864

commit v6 on v5

--- a/solution.py
+++ b/solution.py
@@ -397,9 +397,7 @@
             halo_copy(layer).start()
 
     def convolve(layer, part):
-        start, count = parts_of(layer)[part]
-        if start == 0:
-
+        def wait_halo():
             @pl.when(first)
             def _():
                 EXT[layer, pl.ds(0, halo), :] = jnp.zeros((halo, Cn), BF16)
@@ -440,7 +438,13 @@
                 jnp.sum(conved * conved, axis=1, keepdims=True),
             )
 
-        each_chunk(body, start, count)
+        if layer == 0:
+            wait_halo()
+            each_chunk(body)
+        else:
+            each_chunk(body, CHUNK, rows - CHUNK)
+            wait_halo()
+            each_chunk(body, 0, CHUNK)
         send_stat(2 * layer + 1, part)
 
     def mix(layer, part):
@@ -843,10 +847,12 @@
             far_take(fore(out))
             mix(layer, 0)
             for k in range(3):
-                branch(layer, k, every, select=leaves, together=True)
-            far_take(aft(out)[:1])
+                branch(layer, k, every, late=False, select=leaves)
             for k in range(3, S):
                 branch(layer, k, every, late=False, only=head_columns, select=leaves)
+            far_take(aft(out)[:1])
+            for k in range(1, 3):
+                branch(layer, k, every, early=False, select=leaves)
             far_take(aft(out)[1:])
             for k in range(3):
                 branch(layer, k, every, select=stays, together=True)

time: 183 us -> 180 us (0.984)
  Pallas kernels: 180 us -> 177 us
    pallas_call x1, Pallas kernels: 180 us -> 177 us  [shards(): pl.pallas_call(functools.partial(kernel, S, T), out_shape=jax.ShapeDtypeS...]
where the time goes in v6:
time: 180 us; the launch traced here: 179 us
  Pallas kernels  177 us (98%)
  local copies, waits for them, and re-layouts  2.06 us (1%)
    pallas_call x1, Pallas kernels, shards(): pl.pallas_call(functools.partial(kernel, S, T), out_shape=jax.ShapeDtypeS...  177 us

profile of v6, /device:TPU:3, one launch (start us, length us, event | category | flops | bytes accessed | tf_op | source)
XLA Modules:
  0.0 179.5 jit_solution(11128826934054809584)
XLA Ops:
  0.0 177.4 %shard_map.82 = bf16[384,1024]{1,0:T(8,128)(2,1)} custom-call(bf16[384,1024]{1,0:T(8,128)(2,1)} %h_ref.1, f32[2,1024]{1,0:T(2,128)} %gain_ref.1, bf16[2,1024,512]{2,1,0:T(8,128)(2,1)} %wv_ref.1, bf16[2,1024,512]{2,1,0:T(8,128)(2,1)} %wg_ref.1, f32[31,2,512]{2,1,0:T(2,128)} %bitcast.1, f32[2,512]{1,0:T(2,128)} %ng_ref.1, f32[2,512]{1,0:T(2,128)} %ns_ref.1, ...), custom_call_target="tpu_custom_call" | custom-call | tf_op jit(solution)/shard_map/pallas_call | solution.py:991
  177.4 2.1 %copy.10 = bf16[384,1024]{1,0:T(8,128)(2,1)} copy(bf16[384,1024]{1,0:T(8,128)(2,1)} %shard_map.82) | data formatting | bytes 1572864

commit v7 on v6

--- a/solution.py
+++ b/solution.py
@@ -15,7 +15,7 @@
 def cuts(Ds, layer):
     if Ds < 512:
         return (1, 1, 1)
-    return (2, 2, 2) if layer == 0 else (2, 4, 4)
+    return (2, 2, 4) if layer == 0 else (4, 4, 4)
 
 
 def kernel(
@@ -983,7 +983,7 @@
     chips = T // 2
     halo = (conv_taps.shape[1] - 1 + 15) // 16 * 16
     items = sum(sum(cuts(Ds, layer)) for layer in range(L))
-    Q = 2 * cuts(Ds, 0)[2]
+    Q = max(2, cuts(Ds, 0)[2])
     fine = Q if S == T else 1
     vmem = pl.BlockSpec(memory_space=pltpu.VMEM)
     hbm = pl.BlockSpec(memory_space=pl.ANY)

time: 180 us -> 180 us (level)
  no operation moved by 1% of the time
where the time goes in v7:
time: 180 us; the launch traced here: 178 us
  Pallas kernels  176 us (98%)
  local copies, waits for them, and re-layouts  2.06 us (1%)
    pallas_call x1, Pallas kernels, shards(): pl.pallas_call(functools.partial(kernel, S, T), out_shape=jax.ShapeDtypeS...  176 us

profile of v7, /device:TPU:3, one launch (start us, length us, event | category | flops | bytes accessed | tf_op | source)
XLA Modules:
  0.0 178.4 jit_solution(12388591344760316791)
XLA Ops:
  0.0 176.3 %shard_map.82 = bf16[384,1024]{1,0:T(8,128)(2,1)} custom-call(bf16[384,1024]{1,0:T(8,128)(2,1)} %h_ref.1, f32[2,1024]{1,0:T(2,128)} %gain_ref.1, bf16[2,1024,512]{2,1,0:T(8,128)(2,1)} %wv_ref.1, bf16[2,1024,512]{2,1,0:T(8,128)(2,1)} %wg_ref.1, f32[31,2,512]{2,1,0:T(2,128)} %bitcast.1, f32[2,512]{1,0:T(2,128)} %ng_ref.1, f32[2,512]{1,0:T(2,128)} %ns_ref.1, ...), custom_call_target="tpu_custom_call" | custom-call | tf_op jit(solution)/shard_map/pallas_call | solution.py:991
  176.3 2.1 %copy.10 = bf16[384,1024]{1,0:T(8,128)(2,1)} copy(bf16[384,1024]{1,0:T(8,128)(2,1)} %shard_map.82) | data formatting | bytes 1572864
